TPU v7x, 32 devices: a whole 2x2x4 slice. The times are simulated.
32 devices in a mesh: ep: 8 (over z, y), tp: 4 (over x, core).
Axes of the slice: x: 2, y: 2, z: 4, core: 2. Of those that a mesh axis runs over, the one named last changes fastest.
Arguments:
- tokens: bfloat16 [256, 2048], P('ep'), may hold values from -6 to 6
- kv_cache: bfloat16 [256, 1024, 512], P('ep', None, 'tp'), may hold values from -320 to 320
- lengths: int32 [256], P('ep'), may hold values from 1 to 1024, 131072 in all
- attn_gain: float32 [2048], replicated, may hold values from 0.1 to 1.9
- w_query: bfloat16 [2048, 1024], P(None, 'tp'), may hold values from -0.125 to 0.125
- w_key: bfloat16 [2048, 256], P(None, 'tp'), may hold values from -0.125 to 0.125
- w_value: bfloat16 [2048, 256], P(None, 'tp'), may hold values from -0.125 to 0.125
- lambdas: float32 [16], P('tp'), may hold values from 0.3 to 0.8
- head_gain: float32 [64], replicated, may hold values from 0.1 to 1.9
- w_out: bfloat16 [1024, 2048], replicated, may hold values from -0.1875 to 0.1875
- ffn_gain: float32 [2048], replicated, may hold values from 0.1 to 1.9
- w_shared_gate: bfloat16 [2048, 512], P(None, 'tp'), may hold values from -0.125 to 0.125
- w_shared_up: bfloat16 [2048, 512], P(None, 'tp'), may hold values from -0.125 to 0.125
- w_shared_down: bfloat16 [512, 2048], P('tp'), may hold values from -0.25 to 0.25
- routing: int32 [256, 4], replicated, may hold values from 0 to 31, all different within a row; in each aligned block of 32 rows (0 to 31, 32 to 63, ...) at most 8 rows name the same one
- route_weights: float32 [256, 4], P('ep'), may hold values from 0.1 to 1
- w_exp_gate: bfloat16 [32, 2048, 512], P(('ep', 'tp')), may hold values from -0.125 to 0.125
- w_exp_up: bfloat16 [32, 2048, 512], P(('ep', 'tp')), may hold values from -0.125 to 0.125
- w_exp_down: bfloat16 [32, 512, 2048], P(('ep', 'tp')), may hold values from -0.25 to 0.25
Outputs:
- mixed: bfloat16 [256, 2048], P('ep', 'tp')
Inputs may be any that keep to these rules, and one draw needn't show every extreme that they name: `lengths`: A sequence's cache holds its past keys and values at positions below its length, and the new token follows them; some sequence uses all 1024 positions. `routing`: each row names 4 different experts. Within the rows of one group of 32 sequences (aligned blocks) no expert is named by more than 8 rows, and in some blocks an expert is named by exactly 8.
All inputs are finite; a program needn't handle non-finite values. No bound on the sum of `lengths` on one device may be relied on, other than what follows from the above.
Results may differ from a plain program's by a relative error of at most 0.015.
The roundings to bfloat16 on the way count: a program that leaves them out, or rounds other values in their place, can miss the bound.
Values may be sent and summed in bfloat16 or wider, within the bound.
No kernel may reach another device: no remote copies, remote signals or barrier semaphores. Data moves between devices by JAX's collectives and lax.ppermute only.
A program may use at most 128 MiB of HBM per device.

v0:
```python
import jax
import jax.numpy as jnp
from jax import lax
from jax.sharding import PartitionSpec as P

epsilon = 1e-06
neg_fill = -1e30


def norm_rows(values, gain_vec):
    widened = values.astype(jnp.float32)
    return (
        widened
        * lax.rsqrt(jnp.mean(widened * widened, axis=-1, keepdims=True) + epsilon)
        * gain_vec
    )


def attention(normed, kv_cache, lengths, w_query, w_key, w_value, lambdas, head_gain):
    seq_count = normed.shape[0]
    v_width = head_gain.shape[0]
    qk_width = v_width // 2
    kv_local = kv_cache.shape[2] // (2 * v_width)
    head_local = lambdas.shape[0]
    group_size = head_local // kv_local
    cache_len = kv_cache.shape[1]
    queries = jnp.dot(normed, w_query, preferred_element_type=jnp.float32).astype(jnp.bfloat16)
    queries = queries.reshape(seq_count, kv_local, group_size, 2, qk_width)
    key_new = jnp.dot(normed, w_key, preferred_element_type=jnp.float32).astype(jnp.bfloat16)
    key_new = key_new.reshape(seq_count, kv_local, 2, qk_width)
    value_new = jnp.dot(normed, w_value, preferred_element_type=jnp.float32).astype(jnp.bfloat16)
    value_new = value_new.reshape(seq_count, kv_local, v_width)
    layout = kv_cache.reshape(seq_count, cache_len, kv_local, 2 * v_width)
    keys_old = layout[..., :v_width].reshape(seq_count, cache_len, kv_local, 2, qk_width)
    values_old = layout[..., v_width:]
    scaling = qk_width ** (-0.5)
    scores_old = (
        jnp.einsum("skgmd,sckmd->skgmc", queries, keys_old, preferred_element_type=jnp.float32)
        * scaling
    )
    scores_new = (
        jnp.einsum("skgmd,skmd->skgm", queries, key_new, preferred_element_type=jnp.float32)
        * scaling
    )
    position = jnp.arange(cache_len, dtype=jnp.int32)
    valid_mask = (position[None, :] < lengths[:, None])[:, None, None, None, :]
    scores_old = jnp.where(valid_mask, scores_old, neg_fill)
    highest = jnp.maximum(jnp.max(scores_old, axis=-1), scores_new)
    expo_old = jnp.where(valid_mask, jnp.exp(scores_old - highest[..., None]), 0.0)
    expo_new = jnp.exp(scores_new - highest)
    totals = jnp.sum(expo_old, axis=-1) + expo_new
    lambda_grid = lambdas.reshape(kv_local, group_size)[None, :, :]
    weight_old = (
        expo_old[..., 0, :] / totals[..., 0, None]
        - lambda_grid[..., None] * expo_old[..., 1, :] / totals[..., 1, None]
    ).astype(jnp.bfloat16)
    weight_new = (
        expo_new[..., 0] / totals[..., 0] - lambda_grid * expo_new[..., 1] / totals[..., 1]
    ).astype(jnp.bfloat16)
    head_mix = jnp.einsum(
        "skgc,sckv->skgv", weight_old, values_old, preferred_element_type=jnp.float32
    )
    head_mix = (
        head_mix
        + weight_new.astype(jnp.float32)[..., None] * value_new.astype(jnp.float32)[:, :, None, :]
    )
    return (
        norm_rows(head_mix, head_gain).astype(jnp.bfloat16).reshape(seq_count, head_local * v_width)
    )


def shards(
    tokens,
    kv_cache,
    lengths,
    attn_gain,
    w_query,
    w_key,
    w_value,
    lambdas,
    head_gain,
    w_out,
    ffn_gain,
    w_shared_gate,
    w_shared_up,
    w_shared_down,
    routing,
    route_weights,
    w_exp_gate,
    w_exp_up,
    w_exp_down,
):
    seq_count = tokens.shape[0]
    width = tokens.shape[1]
    tp_count = lax.axis_size("tp")
    tp_index = lax.axis_index("tp")
    ep_count = lax.axis_size("ep")
    ep_index = lax.axis_index("ep")
    normed = norm_rows(tokens, attn_gain).astype(jnp.bfloat16)
    head_out = attention(normed, kv_cache, lengths, w_query, w_key, w_value, lambdas, head_gain)
    share_rows = head_out.shape[1]
    all_heads = lax.all_gather(head_out, "tp", axis=1, tiled=True)
    pieces = jnp.einsum(
        "stk,tkd->tsd",
        all_heads.reshape(seq_count, tp_count, share_rows),
        w_out.reshape(tp_count, share_rows, -1),
        preferred_element_type=jnp.float32,
    )
    rounded = lax.optimization_barrier(pieces.astype(jnp.bfloat16))
    projected = jnp.sum(rounded.astype(jnp.float32), axis=0)
    residual = (tokens.astype(jnp.float32) + projected).astype(jnp.bfloat16)
    ffn_in = norm_rows(residual, ffn_gain).astype(jnp.bfloat16)
    gate_vals = jnp.dot(ffn_in, w_shared_gate, preferred_element_type=jnp.float32)
    up_vals = jnp.dot(ffn_in, w_shared_up, preferred_element_type=jnp.float32)
    shared_act = (jax.nn.silu(gate_vals) * up_vals).astype(jnp.bfloat16)
    shared_part = jnp.dot(shared_act, w_shared_down, preferred_element_type=jnp.float32)
    top_count = routing.shape[1]
    experts = w_exp_gate.shape[0] * ep_count * tp_count
    capacity = max(2, 2 * seq_count * top_count // experts)
    own_routing = lax.dynamic_slice_in_dim(routing, ep_index * seq_count, seq_count, 0)
    flat_ids = own_routing.reshape(-1)
    onehot = (flat_ids[:, None] == jnp.arange(experts, dtype=jnp.int32)[None, :]).astype(jnp.int32)
    slot_rank = jnp.sum((jnp.cumsum(onehot, axis=0) - onehot) * onehot, axis=1)
    in_column = flat_ids % tp_count == tp_index
    slot_ids = jnp.where(in_column, flat_ids // tp_count * capacity + slot_rank, -1)
    selector = (
        slot_ids[:, None] == jnp.arange(ep_count * capacity, dtype=jnp.int32)[None, :]
    ).astype(jnp.bfloat16)
    dispatch = jnp.sum(selector.reshape(seq_count, top_count, -1), axis=1)
    packed = jnp.einsum("sj,sd->jd", dispatch, ffn_in, preferred_element_type=jnp.float32).astype(
        jnp.bfloat16
    )
    packed = packed.reshape(ep_count, capacity, width)
    arrived = lax.all_to_all(packed, "ep", split_axis=0, concat_axis=0, tiled=True)
    flat_rows = arrived.reshape(-1, width)
    gate_part = jnp.dot(flat_rows, w_exp_gate[0], preferred_element_type=jnp.float32)
    up_part = jnp.dot(flat_rows, w_exp_up[0], preferred_element_type=jnp.float32)
    inner_act = (jax.nn.silu(gate_part) * up_part).astype(jnp.bfloat16)
    result = jnp.dot(inner_act, w_exp_down[0], preferred_element_type=jnp.float32).astype(
        jnp.bfloat16
    )
    computed = result.reshape(arrived.shape)
    returned = lax.all_to_all(computed, "ep", split_axis=0, concat_axis=0, tiled=True)
    routed_rows = jnp.dot(
        selector, returned.reshape(ep_count * capacity, width), preferred_element_type=jnp.float32
    ).reshape(seq_count, top_count, width)
    routed_part = jnp.sum(route_weights[:, :, None] * routed_rows, axis=1)
    combined = lax.psum_scatter(
        (shared_part + routed_part).astype(jnp.bfloat16), "tp", scatter_dimension=1, tiled=True
    ).astype(jnp.float32)
    width_share = width // tp_count
    own_resid = lax.dynamic_slice_in_dim(residual, tp_index * width_share, width_share, 1).astype(
        jnp.float32
    )
    return (own_resid + combined).astype(jnp.bfloat16)


def solution(mesh):
    return jax.shard_map(
        shards,
        mesh=mesh,
        in_specs=(
            P("ep", None),
            P("ep", None, "tp"),
            P("ep"),
            P(),
            P(None, "tp"),
            P(None, "tp"),
            P(None, "tp"),
            P("tp"),
            P(),
            P(),
            P(),
            P(None, "tp"),
            P(None, "tp"),
            P("tp", None),
            P(),
            P("ep", None),
            P(("ep", "tp"), None, None),
            P(("ep", "tp"), None, None),
            P(("ep", "tp"), None, None),
        ),
        out_specs=P("ep", "tp"),
        check_vma=False,
    )
```

profile of v0, /device:TPU:0, one launch (start us, length us, event | category | flops | bytes accessed | tf_op | source)
XLA Modules:
  0.0 108.7 jit_solution(12720334476326230259)
XLA Ops:
  6.5 1.2 %fusion.30 = f32[32]{0:T(128)S(1)} fusion(bf16[32,2048]{1,0:T(8,128)(2,1)} %param.19), kind=kLoop, calls=%fused_computation.44 | loop fusion | flops 196576 | bytes 131200 | tf_op jit(solution)/shard_map/reduce_sum | solution.py:14
  7.7 1.6 %convolution_convert_fusion.3 = bf16[32,256]{1,0:T(8,128)(2,1)S(1)} fusion(bf16[2048,256]{1,0:T(8,128)(2,1)} %param.23, bf16[32,2048]{1,0:T(8,128)(2,1)} %param.19, f32[2048]{0:T(1024)} %param.22, f32[32]{0:T(128)S(1)} %add_rsqrt_fusion.2), kind=kOutput, calls=%fused_computation.23 | convolution fusion | flops 33824768 | bytes 1204352 | tf_op jit(solution)/shard_map/dot_general | solution.py:27
  9.5 11.9 %copy.64 = bf16[32,1024,128]{1,2,0:T(8,128)(2,1)} copy(bf16[32,1024,128]{2,1,0:T(8,128)(2,1)} %param.20) | data formatting | bytes 16777216 | tf_op args[1]
  21.4 2.6 %slice.34 = bf16[32,1024,1,64]{1,3,0,2:T(8,128)(2,1)S(1)} slice(bf16[32,1024,1,128]{1,3,0,2:T(8,128)(2,1)} %bitcast.130), slice={[0:32], [0:1024], [0:1], [0:64]} | slice | bytes 8388608 | tf_op jit(solution)/shard_map/slice | solution.py:34
  24.2 1.0 fusion.88
  25.3 1.2 %convolution_convert_fusion.5 = bf16[32,64]{1,0:T(8,128)(2,1)S(1)} fusion(bf16[2048,64]{0,1:T(8,128)(2,1)} %param.24, bf16[32,2048]{1,0:T(8,128)(2,1)S(1)} %copy-done.1, f32[2048]{0:T(1024)S(1)} %copy-done.4, f32[32]{0:T(128)S(1)} %add_rsqrt_fusion.2), kind=kOutput, calls=%fused_computation.28 | convolution fusion | flops 8652800 | bytes 405632 | tf_op jit(solution)/shard_map/dot_general | solution.py:29
  26.6 0.2 fusion.53
  27.0 1.7 %fusion.87 = (f32[32,4,2]{1,2,0:T(2,128)S(1)}, f32[32,1,4,2,1024]{4,2,3,0,1:T(4,128)}) fusion(f32[32,1,4,2,1024]{4,2,3,0,1:T(4,128)S(1)} %get-tuple-element.15, f32[32,4,2]{1,2,0:T(2,128)S(1)} %copy.67, pred[32,1024]{1,0:T(8,128)(4,1)S(1)} %iota_compare_fusion), kind=kLoop, calls=%fused_computation.117 | loop fusion | flops 786176 | bytes 2131968 | tf_op jit(solution)/shard_map/reduce_sum | solution.py:51
  29.2 1.2 %fusion.21 = f32[32,64]{1,0:T(8,128)S(1)} fusion(bf16[2048,64]{0,1:T(8,128)(2,1)} %param.25, bf16[32,2048]{1,0:T(8,128)(2,1)S(1)} %copy-done.1, f32[2048]{0:T(1024)S(1)} %copy-done.4, f32[32]{0:T(128)S(1)} %add_rsqrt_fusion.2), kind=kOutput, calls=%fused_computation.27 | convolution fusion | flops 8654848 | bytes 409728 | tf_op jit(solution)/shard_map/dot_general | solution.py:31
  30.4 3.9 %multiply_reduce_fusion = (f32[32,4]{1,0:T(8,128)S(1)}, f32[32,4,64]{2,1,0:T(4,128)S(1)}) fusion(f32[32,64]{1,0:T(8,128)S(1)} %fusion.21, f32[32,4]{1,0:T(8,128)S(1)} %copy.72, bf16[32,1024,1,128]{1,3,0,2:T(8,128)(2,1)} %bitcast.131, f32[32,1,4,2,1024]{4,2,3,0,1:T(4,128)} %get-tuple-element.10, f32[32,4]{1,0:T(8,128)S(1)} %copy.71, f32[4]{0:T(128)S(1)} %copy-done.8, ...), kind=kOutput, calls=%fused_computation.70 | convolution fusion | flops 17465216 | bytes 5285904 | tf_op jit(solution)/shard_map/skgc,sckv->skgv/dot_general | solution.py:60
  34.5 6.2 %all_gather.3 = bf16[32,1024]{1,0:T(8,128)(2,1)S(1)} all-gather(bf16[32,256]{1,0:T(8,128)(2,1)S(1)} %reshape.256), channel_id=1, replica_groups=mesh['ep'=8,'tp'=4] {'tp'}, dimensions={1}, use_global_device_ids=true | all-gather | bytes 81920 | tf_op jit(solution)/shard_map/all_gather | solution.py:102
  40.8 3.0 %convolution_convert_fusion = bf16[4,32,2048]{2,1,0:T(8,128)(2,1)S(1)} fusion(bf16[4,256,2048]{2,1,0:T(8,128)(2,1)} %bitcast.133, bf16[4,4,8,256]{3,2,1,0:T(8,128)(2,1)S(1)} %bitcast.134), kind=kOutput, calls=%fused_computation.3 | convolution fusion | flops 134479872 | bytes 4784128 | tf_op jit(solution)/shard_map/stk,tkd->tsd/dot_general | solution.py:103
  44.4 0.2 reduce_window_sum.11
  45.1 0.3 fusion.1
  45.4 15.7 %all_to_all.10 = bf16[8,8,2048]{2,1,0:T(8,128)(2,1)S(1)} all-to-all(bf16[8,8,2048]{2,1,0:T(8,128)(2,1)S(1)} %fusion.1), channel_id=1, replica_groups=mesh['ep'=8,'tp'=4] {'ep'}, dimensions={0} | all-to-all | bytes 524288 | tf_op jit(solution)/shard_map/all_to_all | solution.py:134
  61.1 2.1 %fusion.7 = f32[64,512]{1,0:T(8,128)S(1)} fusion(bf16[1,2048,512]{2,1,0:T(8,128)(2,1)} %param.35, bf16[8,8,2048]{2,1,0:T(8,128)(2,1)S(1)} %all_to_all.10), kind=kOutput, calls=%fused_computation.13 | convolution fusion | flops 134217728 | bytes 2490368 | tf_op jit(solution)/shard_map/dot_general | solution.py:136
  63.2 3.2 %fusion.2 = bf16[8,8,2048]{2,1,0:T(8,128)(2,1)} fusion(bf16[1,512,2048]{2,1,0:T(8,128)(2,1)S(1)} %copy-done, bf16[1,2048,512]{2,1,0:T(8,128)(2,1)} %param.36, bf16[8,8,2048]{2,1,0:T(8,128)(2,1)S(1)} %all_to_all.10, f32[64,512]{1,0:T(8,128)S(1)} %fusion.7), kind=kOutput, calls=%fused_computation.7 | convolution fusion | flops 268763136 | bytes 4849664 | tf_op jit(solution)/shard_map/dot_general | solution.py:139
  66.4 3.6 %all-to-all-start.1 = ((bf16[8,8,2048]{2,1,0:T(8,128)(2,1)}), bf16[8,8,2048]{2,1,0:T(8,128)(2,1)S(1)}, u32[]{:S(2)}, u32[]{:S(2)}) async-start(bf16[8,8,2048]{2,1,0:T(8,128)(2,1)} %fusion.2), calls=%async_computation.1 | async-start | bytes 524288 | tf_op jit(solution)/shard_map/all_to_all | solution.py:143
  70.0 0.3 fusion.83
  70.3 8.7 %all-to-all-done.1 = bf16[8,8,2048]{2,1,0:T(8,128)(2,1)S(1)} async-done(((bf16[8,8,2048]{2,1,0:T(8,128)(2,1)}), bf16[8,8,2048]{2,1,0:T(8,128)(2,1)S(1)}, u32[]{:S(2)}, u32[]{:S(2)}) %all-to-all-start.1) | async-done | bytes 262176 | tf_op jit(solution)/shard_map/all_to_all | solution.py:143
  79.0 0.3 fusion.10
  79.3 2.3 %fusion.3 = bf16[32,2048]{1,0:T(8,128)(2,1)} fusion(f32[32,2048]{1,0:T(8,128)S(1)} %fusion.10, bf16[128,2048]{1,0:T(8,128)(2,1)} %param.32, bf16[2048,128]{1,0:T(8,128)(2,1)} %param.31, f32[32,128]{1,0:T(8,128)S(1)} %fusion.83, bf16[32,2048]{1,0:T(8,128)(2,1)S(1)} %get-tuple-element.6, f32[2048]{0:T(1024)S(1)} %copy-done.3, f32[32]{0:T(128)S(1)} %add_rsqrt_fusion.1), kind=kOutput, calls=%fused_computation.9 | convolution fusion | flops 33972224 | bytes 1597568 | tf_op jit(solution)/shard_map/dot_general | solution.py:116
  81.6 18.8 %reduce-scatter.2.cloned.1.call-done = bf16[32,512]{1,0:T(8,128)(2,1)} async-done(((bf16[32,2048]{1,0:T(8,128)(2,1)}), bf16[32,512]{1,0:T(8,128)(2,1)}) %reduce-scatter.2.cloned.1.call-update) | async-done | bytes 32784 | tf_op jit(solution)/shard_map/reduce_scatter | solution.py:148
  100.5 1.4 %add_convert_fusion = bf16[32,512]{1,0:T(8,128)(2,1)} fusion(bf16[32,512]{1,0:T(8,128)(2,1)} %reduce-scatter.2.cloned.1.call-done, bf16[32,2048]{1,0:T(8,128)(2,1)S(1)} %get-tuple-element.6, s32[]{:T(128)S(6)} %select_n.47), kind=kLoop, calls=%fused_computation.62 | loop fusion | flops 65536 | bytes 98308 | tf_op jit(solution)/shard_map/convert_element_type | solution.py:155
  (51 shorter events, 2.4 us)
Async XLA Ops:
  6.5 56.6 %copy-start = (bf16[1,512,2048]{2,1,0:T(8,128)(2,1)S(1)}, bf16[1,512,2048]{2,1,0:T(8,128)(2,1)}, u32[]{:S(2)}) copy-start(bf16[1,512,2048]{2,1,0:T(8,128)(2,1)} %param.37) | copy-start | bytes 6291460
  21.4 2.7 %copy-start.6 = (s32[32]{0:T(128)S(1)}, s32[32]{0:T(128)}, u32[]{:S(2)}) copy-start(s32[32]{0:T(128)} %param.21) | copy-start | bytes 388
  24.1 1.2 %copy-start.1 = (bf16[32,2048]{1,0:T(8,128)(2,1)S(1)}, bf16[32,2048]{1,0:T(8,128)(2,1)}, u32[]{:S(2)}) copy-start(bf16[32,2048]{1,0:T(8,128)(2,1)} %param.19) | copy-start | bytes 393220
  24.1 1.2 %copy-start.4 = (f32[2048]{0:T(1024)S(1)}, f32[2048]{0:T(1024)}, u32[]{:S(2)}) copy-start(f32[2048]{0:T(1024)} %param.22) | copy-start | bytes 24580
  24.2 4.6 %copy-start.8 = (f32[4]{0:T(128)S(1)}, f32[4]{0:T(128)}, u32[]{:S(2)}) copy-start(f32[4]{0:T(128)} %param.26) | copy-start | bytes 52
  30.4 3.9 %copy-start.7 = (f32[64]{0:T(128)S(1)}, f32[64]{0:T(128)}, u32[]{:S(2)}) copy-start(f32[64]{0:T(128)} %param.27) | copy-start | bytes 772
  40.7 3.3 %copy-start.5 = (s32[256,4]{0,1:T(4,128)S(1)}, s32[256,4]{0,1:T(4,128)}, u32[]{:S(2)}) copy-start(s32[256,4]{0,1:T(4,128)} %param.33) | copy-start | bytes 12292
  40.7 4.4 %copy-start.3 = (f32[2048]{0:T(1024)S(1)}, f32[2048]{0:T(1024)}, u32[]{:S(2)}) copy-start(f32[2048]{0:T(1024)} %param.29) | copy-start | bytes 24580
  45.4 24.6 %copy-start.2 = (bf16[2048,128]{1,0:T(8,128)(2,1)S(1)}, bf16[2048,128]{1,0:T(8,128)(2,1)}, u32[]{:S(2)}) copy-start(bf16[2048,128]{1,0:T(8,128)(2,1)} %param.30) | copy-start | bytes 1572868
  61.1 17.9 %copy-start.9 = (f32[32,4]{0,1:T(4,128)S(1)}, f32[32,4]{0,1:T(4,128)}, u32[]{:S(2)}) copy-start(f32[32,4]{0,1:T(4,128)} %param.34) | copy-start | bytes 1540
  66.4 12.6 %all-to-all-start.1 = ((bf16[8,8,2048]{2,1,0:T(8,128)(2,1)}), bf16[8,8,2048]{2,1,0:T(8,128)(2,1)S(1)}, u32[]{:S(2)}, u32[]{:S(2)}) async-start(bf16[8,8,2048]{2,1,0:T(8,128)(2,1)} %fusion.2), calls=%async_computation.1 | async-start | bytes 524288 | tf_op jit(solution)/shard_map/all_to_all | solution.py:143
  70.0 30.5 %reduce-scatter.2.cloned.1.call-start = ((), (), s32[]{:S(2)}) async-start(), calls=%async_computation.3 | async-start | bytes 163840 | tf_op jit(solution)/shard_map/reduce_scatter | solution.py:148
Sparse Core Ops, SparseCore 0:
  81.8 18.6 reduce-scatter.1
where the time goes:
time: 110 us; the launch traced here: 109 us
  waiting for transfers between devices  27.5 us (25%)
  blocking collectives  21.9 us (20%)
  matrix products  20.6 us (19%)
  local copies, waits for them, and re-layouts  16.1 us (15%)
  between operations  13.6 us (12%)
  other arithmetic  5.36 us (5%)
  starting transfers between devices  3.62 us (3%)
    reduce_scatter x1, waiting for transfers between devices, shards(): lax.psum_scatter((shared_part + routed_part).astype(jnp.bfloat16), 'tp',...  18.8 us
    all_to_all x1, blocking collectives, shards(): lax.all_to_all(packed, 'ep', split_axis=0, concat_axis=0, tiled=True)  15.7 us
    unnamed x22, local copies, waits for them, and re-layouts  12.1 us
    all_to_all x1, waiting for transfers between devices, shards(): lax.all_to_all(computed, 'ep', split_axis=0, concat_axis=0, tiled=True)  8.68 us
    all_gather x1, blocking collectives, shards(): all_heads = lax.all_gather(head_out, 'tp', axis=1, tiled=True)  6.22 us
    dot_general x1, matrix products, attention(): jnp.einsum('skgc,sckv->skgv', weight_old, values_old, preferred_element_t...  3.87 us
    all_to_all x1, starting transfers between devices, shards(): lax.all_to_all(computed, 'ep', split_axis=0, concat_axis=0, tiled=True)  3.59 us
    dot_general x1, matrix products, shards(): jnp.dot(inner_act, w_exp_down[0], preferred_element_type=jnp.float32)  3.2 us
  transfers between devices with their start and end apart: 2, of which 2 were waited for; matrix products, arithmetic and copies ran while one was open for 0% of the time, Pallas kernels for 0%

commit v1 on v0

v1 whole, which is shorter than its diff:
```python
import functools

import jax
import jax.numpy as jnp
from jax import lax
from jax.experimental import pallas as pl
from jax.experimental.pallas import tpu as pltpu
from jax.sharding import PartitionSpec as P

epsilon = 1e-06
neg_fill = -1e30
f32 = jnp.float32
bf16 = jnp.bfloat16
VMEM = pl.BlockSpec(memory_space=pltpu.VMEM)
SMEM = pl.BlockSpec(memory_space=pltpu.SMEM)


def iota(shape, axis):
    return lax.broadcasted_iota(jnp.int32, shape, axis)


def dot(a, b):
    return jnp.dot(a, b, preferred_element_type=f32)


def inv_rms(values):
    return lax.rsqrt(jnp.mean(values * values, axis=-1, keepdims=True) + epsilon)


def slots_of(routing, experts, capacity):
    rows, top_count = routing.shape
    ids = iota((rows, experts), 1)
    hits = [routing[:, k : k + 1] == ids for k in range(top_count)]
    present = jnp.zeros((rows, experts), f32)
    for hit in hits:
        present = jnp.where(hit, 1.0, present)
    earlier = (iota((rows, rows), 1) < iota((rows, rows), 0)).astype(bf16)
    before = dot(earlier, present.astype(bf16))
    ranks = [jnp.sum(jnp.where(hit, before, 0.0), axis=1, keepdims=True) for hit in hits]
    return [
        routing[:, k : k + 1] * capacity + ranks[k].astype(jnp.int32) for k in range(top_count)
    ]


def attention_kernel(
    capacity,
    experts,
    lengths_ref,
    place_ref,
    lambdas_ref,
    tokens_ref,
    attn_gain_ref,
    w_query_ref,
    w_key_ref,
    w_value_ref,
    head_gain_ref,
    routing_ref,
    kv_ref,
    heads_ref,
    send_ref,
    q_scr,
    k_scr,
    v_scr,
    o_scr,
):
    step = pl.program_id(0)
    seqs, rows, lanes = q_scr.shape
    heads = rows // 2
    v_width = lanes // 2
    qk_width = v_width // 2
    block, cache_len, _ = kv_ref.shape
    scaling = qk_width ** (-0.5)

    @pl.when(step == 0)
    def _():
        tokens = tokens_ref[...].astype(f32)
        normed = (tokens * inv_rms(tokens) * attn_gain_ref[...]).astype(bf16)
        queries = dot(normed, w_query_ref[...]).astype(bf16).astype(f32)
        pad = jnp.zeros((seqs, v_width), f32)
        k_scr[...] = jnp.concatenate(
            [dot(normed, w_key_ref[...]).astype(bf16).astype(f32), pad], axis=1
        )
        v_scr[...] = jnp.concatenate(
            [pad, dot(normed, w_value_ref[...]).astype(bf16).astype(f32)], axis=1
        )
        lane = iota((seqs, lanes), 1)
        for h in range(heads):
            pair = queries[:, (h // 2) * lanes : (h // 2 + 1) * lanes]
            if h % 2:
                pair = pltpu.roll(pair, v_width, 1)
            for m in range(2):
                keep = (lane >= m * qk_width) & (lane < (m + 1) * qk_width)
                q_scr[:, m * heads + h, :] = jnp.where(keep, pair, 0.0)

    row = iota((rows, 1), 0)
    sign = jnp.where(row < heads, 1.0, 0.0)
    for h in range(heads):
        sign = jnp.where(row == heads + h, -lambdas_ref[h], sign)
    position = iota((rows, cache_len), 1)
    for b in range(block):
        s = step * block + b
        q = q_scr[s]
        cache = kv_ref[b]
        scores = (
            lax.dot_general(
                q.astype(bf16), cache, (((1,), (1,)), ((), ())), preferred_element_type=f32
            )
            * scaling
        )
        scores = jnp.where(position < lengths_ref[s], scores, neg_fill)
        fresh = jnp.sum(q * k_scr[pl.ds(s, 1), :], axis=1, keepdims=True) * scaling
        top = jnp.maximum(jnp.max(scores, axis=1, keepdims=True), fresh)
        expo = jnp.exp(scores - top)
        expo_new = jnp.exp(fresh - top)
        factor = sign / (jnp.sum(expo, axis=1, keepdims=True) + expo_new)
        part = expo * factor
        weights = (part + pltpu.roll(part, heads, 0)).astype(bf16)
        part_new = jnp.broadcast_to(expo_new * factor, (rows, lanes))
        weight_new = (part_new + pltpu.roll(part_new, heads, 0)).astype(bf16).astype(f32)
        o_scr[s] = dot(weights, cache) + weight_new * v_scr[pl.ds(s, 1), :]

    @pl.when(step == pl.num_programs(0) - 1)
    def _():
        lane = iota((seqs, lanes), 1)
        outs = []
        for h in range(heads):
            mix = jnp.where(lane >= v_width, o_scr[:, h, :], 0.0)
            mean = jnp.sum(mix * mix, axis=1, keepdims=True) * (1.0 / v_width)
            outs.append(mix * lax.rsqrt(mean + epsilon) * head_gain_ref[...])
        pairs = [
            jnp.where(lane < v_width, pltpu.roll(outs[2 * p], v_width, 1), outs[2 * p + 1])
            for p in range(heads // 2)
        ]
        head_out = jnp.concatenate(pairs, axis=1).astype(bf16)
        heads_ref[...] = head_out
        slots = slots_of(routing_ref[...], experts, capacity)
        ids = iota((seqs, experts * capacity), 1)
        picks = jnp.zeros((seqs, experts * capacity), f32)
        for slot in slots:
            picks = jnp.where(slot == ids, 1.0, picks)
        picks = picks.T.astype(bf16)
        width = head_out.shape[1]
        share = send_ref.shape[1] - width
        send_ref[:, :width] = dot(picks, head_out).astype(bf16)
        own = tokens_ref[:, pl.ds(pl.multiple_of(place_ref[0] * share, share), share)]
        send_ref[:, width:] = dot(picks, own).astype(bf16)


def expert_kernel(
    direct,
    arrived_ref,
    heads_ref,
    tokens_ref,
    w_out_ref,
    ffn_gain_ref,
    w_gate_ref,
    w_up_ref,
    w_down_ref,
    send_ref,
    ffn_ref,
    residual_ref,
    res_scr,
):
    groups, chunk, packed = arrived_ref.shape
    tp_count, seqs, width = heads_ref.shape
    capacity = chunk // tp_count
    rows = groups * capacity
    share = packed - width
    lefts = []
    tokens = []
    for j in range(tp_count):
        piece = arrived_ref[:, j * capacity : (j + 1) * capacity, :].astype(f32)
        piece = piece.reshape(rows, packed)
        lefts.append(jnp.concatenate([piece[:, :width].astype(bf16), heads_ref[j]], axis=0))
        own = tokens_ref[:, j * share : (j + 1) * share].astype(f32)
        tokens.append(jnp.concatenate([piece[:, width:], own], axis=0))
    square = jnp.zeros((rows + seqs, 1), f32)
    for n in range(tp_count):
        total = jnp.zeros((rows + seqs, share), f32)
        for j in range(tp_count):
            part = dot(
                lefts[j], w_out_ref[j * width : (j + 1) * width, n * share : (n + 1) * share]
            )
            total = total + part.astype(bf16).astype(f32)
        residual = (tokens[n] + total).astype(bf16)
        residual_ref[:, n * share : (n + 1) * share] = residual[rows:]
        residual = residual.astype(f32)
        res_scr[:, n * share : (n + 1) * share] = residual
        square = square + jnp.sum(residual * residual, axis=1, keepdims=True)
    scale = lax.rsqrt(square * (1.0 / res_scr.shape[1]) + epsilon)
    ffn_in = (res_scr[...] * scale * ffn_gain_ref[...]).astype(bf16)
    ffn_ref[...] = ffn_in[rows:]
    flat_rows = ffn_in[:rows]
    gate = dot(flat_rows, w_gate_ref[...])
    up = dot(flat_rows, w_up_ref[...])
    act = (gate / (1.0 + jnp.exp(-gate)) * up).astype(bf16)
    for j in range(tp_count):
        result = dot(act, w_down_ref[:, j * share : (j + 1) * share])
        if direct:
            for i in range(groups):
                send_ref[(i * tp_count + j) * capacity : (i * tp_count + j + 1) * capacity, :] = (
                    result[i * capacity : (i + 1) * capacity].astype(bf16)
                )
        else:
            send_ref[:, j * share : (j + 1) * share] = result.astype(bf16)


def shared_kernel(ffn_ref, w_gate_ref, w_up_ref, w_down_ref, part_ref):
    tp_count, _, share = part_ref.shape
    ffn_in = ffn_ref[...]
    gate = dot(ffn_in, w_gate_ref[...])
    up = dot(ffn_in, w_up_ref[...])
    act = (gate / (1.0 + jnp.exp(-gate)) * up).astype(bf16)
    for j in range(tp_count):
        part_ref[j] = dot(act, w_down_ref[:, j * share : (j + 1) * share]).astype(bf16)


def combine_kernel(
    capacity, experts, place_ref, residual_ref, part_ref, returned_ref, routing_ref, rates_ref, out_ref
):
    seqs, share = out_ref.shape
    slots = slots_of(routing_ref[...], experts, capacity)
    ids = iota((seqs, experts * capacity), 1)
    mixing = jnp.zeros((seqs, experts * capacity), f32)
    for k, slot in enumerate(slots):
        mixing = jnp.where(slot == ids, rates_ref[:, k : k + 1], mixing)
    high = mixing.astype(bf16)
    low = (mixing - high.astype(f32)).astype(bf16)
    returned = returned_ref[...]
    routed = dot(high, returned) + dot(low, returned)
    own = residual_ref[:, pl.ds(pl.multiple_of(place_ref[0] * share, share), share)].astype(f32)
    shared = jnp.zeros((seqs, share), f32)
    for j in range(part_ref.shape[0]):
        shared = shared + part_ref[j].astype(f32)
    out_ref[...] = (own + shared + routed).astype(bf16)


def params(mib, **more):
    return pltpu.CompilerParams(vmem_limit_bytes=mib << 20, **more)


def shards(
    tokens,
    kv_cache,
    lengths,
    attn_gain,
    w_query,
    w_key,
    w_value,
    lambdas,
    head_gain,
    w_out,
    ffn_gain,
    w_shared_gate,
    w_shared_up,
    w_shared_down,
    routing,
    route_weights,
    w_exp_gate,
    w_exp_up,
    w_exp_down,
):
    seqs, width = tokens.shape
    tp_count = lax.axis_size("tp")
    tp_index = lax.axis_index("tp")
    ep_count = lax.axis_size("ep")
    ep_index = lax.axis_index("ep")
    devices = ep_count * tp_count
    top_count = routing.shape[1]
    experts = w_exp_gate.shape[0] * devices
    capacity = max(2, 2 * seqs * top_count // experts)
    cache_len, lanes = kv_cache.shape[1:]
    v_width = head_gain.shape[0]
    heads = lambdas.shape[0]
    share = width // tp_count
    local = heads * v_width
    packed = local + share
    direct = capacity % 8 == 0
    own_routing = lax.dynamic_slice_in_dim(routing, ep_index * seqs, seqs, 0)
    place = tp_index.reshape(1).astype(jnp.int32)
    gain_row = jnp.concatenate([jnp.zeros((v_width,), f32), head_gain]).reshape(1, lanes)

    block = 4
    whole = lambda shape: pl.BlockSpec(shape, lambda i: (0,) * len(shape))
    head_out, send = pl.pallas_call(
        functools.partial(attention_kernel, capacity, experts),
        grid=(seqs // block,),
        in_specs=[
            SMEM,
            SMEM,
            SMEM,
            whole(tokens.shape),
            whole((1, width)),
            whole(w_query.shape),
            whole(w_key.shape),
            whole(w_value.shape),
            whole((1, lanes)),
            whole(own_routing.shape),
            pl.BlockSpec((block, cache_len, lanes), lambda i: (i, 0, 0)),
        ],
        out_specs=[whole((seqs, local)), whole((devices * capacity, packed))],
        out_shape=[
            jax.ShapeDtypeStruct((seqs, local), bf16),
            jax.ShapeDtypeStruct((devices * capacity, packed), bf16),
        ],
        scratch_shapes=[
            pltpu.VMEM((seqs, 2 * heads, lanes), f32),
            pltpu.VMEM((seqs, lanes), f32),
            pltpu.VMEM((seqs, lanes), f32),
            pltpu.VMEM((seqs, 2 * heads, lanes), f32),
        ],
        compiler_params=params(24),
        cost_estimate=pl.CostEstimate(
            flops=seqs * cache_len * lanes * 32, bytes_accessed=kv_cache.size * 2, transcendentals=0
        ),
        name="attention",
    )(
        lengths,
        place,
        lambdas,
        tokens,
        attn_gain.reshape(1, width),
        w_query,
        w_key,
        w_value,
        gain_row,
        own_routing,
        kv_cache,
    )

    arrived = lax.all_to_all(send, ("ep", "tp"), split_axis=0, concat_axis=0, tiled=True)
    all_heads = lax.all_gather(head_out, "tp", axis=0, tiled=False)

    rows = ep_count * capacity
    if direct:
        arrived = arrived.reshape(ep_count, tp_count * capacity, packed)
        sent_shape = (devices * capacity, share)
    else:
        arrived = arrived.reshape(ep_count, tp_count * capacity, packed)
        sent_shape = (rows, width)
    sent, ffn_own, residual = pl.pallas_call(
        functools.partial(expert_kernel, direct),
        in_specs=[VMEM] * 8,
        out_specs=[VMEM] * 3,
        out_shape=[
            jax.ShapeDtypeStruct(sent_shape, bf16),
            jax.ShapeDtypeStruct((seqs, width), bf16),
            jax.ShapeDtypeStruct((seqs, width), bf16),
        ],
        scratch_shapes=[pltpu.VMEM((rows + seqs, width), f32)],
        compiler_params=params(24),
        cost_estimate=pl.CostEstimate(
            flops=2 * 96 * 10 * (1 << 20), bytes_accessed=10 << 20, transcendentals=0
        ),
        name="experts",
    )(
        arrived,
        all_heads,
        tokens,
        w_out,
        ffn_gain.reshape(1, width),
        w_exp_gate.reshape(w_exp_gate.shape[1:]),
        w_exp_up.reshape(w_exp_up.shape[1:]),
        w_exp_down.reshape(w_exp_down.shape[1:]),
    )
    if not direct:
        sent = sent.reshape(ep_count, capacity, tp_count, share)
        sent = sent.transpose(0, 2, 1, 3).reshape(devices * capacity, share)
    returned = lax.all_to_all(sent, ("ep", "tp"), split_axis=0, concat_axis=0, tiled=True)

    part = pl.pallas_call(
        shared_kernel,
        in_specs=[VMEM] * 4,
        out_specs=VMEM,
        out_shape=jax.ShapeDtypeStruct((tp_count, seqs, share), bf16),
        compiler_params=params(16),
        cost_estimate=pl.CostEstimate(
            flops=2 * 32 * 3 * (1 << 18), bytes_accessed=3 << 19, transcendentals=0
        ),
        name="shared",
    )(ffn_own, w_shared_gate, w_shared_up, w_shared_down)
    parts = lax.all_to_all(part, "tp", split_axis=0, concat_axis=0, tiled=True)

    return pl.pallas_call(
        functools.partial(combine_kernel, capacity, experts),
        in_specs=[SMEM] + [VMEM] * 5,
        out_specs=VMEM,
        out_shape=jax.ShapeDtypeStruct((seqs, share), bf16),
        compiler_params=params(16),
        name="combine",
    )(place, residual, parts, returned, own_routing, route_weights)


def solution(mesh):
    return jax.shard_map(
        shards,
        mesh=mesh,
        in_specs=(
            P("ep", None),
            P("ep", None, "tp"),
            P("ep"),
            P(),
            P(None, "tp"),
            P(None, "tp"),
            P(None, "tp"),
            P("tp"),
            P(),
            P(),
            P(),
            P(None, "tp"),
            P(None, "tp"),
            P("tp", None),
            P(),
            P("ep", None),
            P(("ep", "tp"), None, None),
            P(("ep", "tp"), None, None),
            P(("ep", "tp"), None, None),
        ),
        out_specs=P("ep", "tp"),
        check_vma=False,
    )
```

time: 110 us -> 78.8 us (0.72)
  matrix products: 20.6 us -> 0 us
  Pallas kernels: 0 us -> 19.7 us
  between operations: 13.6 us -> 0.1 us
  blocking collectives: 21.9 us -> 12.4 us
  waiting for transfers between devices: 27.5 us -> 18.3 us
  starting transfers between devices: 3.62 us -> 9.91 us
  other arithmetic: 5.36 us -> 0 us
  local copies, waits for them, and re-layouts: 16.1 us -> 17.8 us
    dot_general x13 -> x0, matrix products: 20.6 us -> none  [the longest x1 3.87 us: attention(): jnp.einsum('skgc,sckv->skgv', weight_old, values_old, preferred_element_t...]
    pallas_call x0 -> x4, Pallas kernels: none -> 19.7 us  [the longest x1 15.1 us: shards(): pl.pallas_call(functools.partial(attention_kernel, capacity, experts), gr...]
    reduce_scatter x1 -> x0, waiting for transfers between devices: 18.8 us -> none  [shards(): lax.psum_scatter((shared_part + routed_part).astype(jnp.bfloat16), 'tp',...]
    all_to_all x1 -> x2, waiting for transfers between devices: 8.68 us -> 18.3 us  [the longest x1 10.5 us: shards(): lax.all_to_all(sent, ('ep', 'tp'), split_axis=0, concat_axis=0, tiled=True)]
    all_to_all x1, blocking collectives: 15.7 us -> 6.99 us  [shards(): parts = lax.all_to_all(part, 'tp', split_axis=0, concat_axis=0, tiled=True)]
    all_to_all x1 -> x2, starting transfers between devices: 3.59 us -> 9.91 us  [the longest x1 7.33 us: shards(): lax.all_to_all(send, ('ep', 'tp'), split_axis=0, concat_axis=0, tiled=True)]
    unnamed x22 -> x40, local copies, waits for them, and re-layouts: 12.1 us -> 17 us
    reduce_sum x6 -> x0, other arithmetic: 3.38 us -> none  [the longest x1 1.7 us: attention(): totals = jnp.sum(expo_old, axis=-1) + expo_new]
where the time goes in v1:
time: 78.8 us; the launch traced here: 78.2 us
  Pallas kernels  19.7 us (25%)
  waiting for transfers between devices  18.3 us (23%)
  local copies, waits for them, and re-layouts  17.8 us (23%)
  blocking collectives  12.4 us (16%)
  starting transfers between devices  9.91 us (13%)
    unnamed x40, local copies, waits for them, and re-layouts  17 us
    pallas_call x1, Pallas kernels, shards(): pl.pallas_call(functools.partial(attention_kernel, capacity, experts), gr...  15.1 us
    all_to_all x1, waiting for transfers between devices, shards(): lax.all_to_all(sent, ('ep', 'tp'), split_axis=0, concat_axis=0, tiled=True)  10.5 us
    all_to_all x1, waiting for transfers between devices, shards(): lax.all_to_all(send, ('ep', 'tp'), split_axis=0, concat_axis=0, tiled=True)  7.87 us
    all_to_all x1, starting transfers between devices, shards(): lax.all_to_all(send, ('ep', 'tp'), split_axis=0, concat_axis=0, tiled=True)  7.33 us
    all_to_all x1, blocking collectives, shards(): parts = lax.all_to_all(part, 'tp', split_axis=0, concat_axis=0, tiled=True)  6.99 us
    all_gather x1, blocking collectives, shards(): all_heads = lax.all_gather(head_out, 'tp', axis=0, tiled=False)  5.37 us
    pallas_call x1, Pallas kernels, shards(): pl.pallas_call(functools.partial(expert_kernel, direct), in_specs=[VMEM]...  2.96 us
  transfers between devices with their start and end apart: 2, of which 2 were waited for; matrix products, arithmetic and copies ran while one was open for 0% of the time, Pallas kernels for 0%

profile of v1, /device:TPU:0, one launch (start us, length us, event | category | flops | bytes accessed | tf_op | source)
XLA Modules:
  0.0 78.2 jit_solution(3950367240598003441)
XLA Ops:
  0.0 0.7 copy-done
  0.9 1.2 %copy.21.w_key_ref = bf16[2048,64]{1,0:T(8,128)(2,1)S(1)} copy(bf16[2048,64]{0,1:T(8,128)(2,1)} %param.24) | data formatting | bytes 524288 | tf_op args[5]
  2.1 1.2 %copy.22.w_value_ref = bf16[2048,64]{1,0:T(8,128)(2,1)S(1)} copy(bf16[2048,64]{0,1:T(8,128)(2,1)} %param.25) | data formatting | bytes 524288 | tf_op args[6]
  3.3 0.7 pad_bitcast_fusion.head_gain_ref
  4.0 3.4 %copy-done.1 = bf16[32,1024,128]{2,1,0:T(8,128)(2,1)S(1)} copy-done((bf16[32,1024,128]{2,1,0:T(8,128)(2,1)S(1)}, bf16[32,1024,128]{2,1,0:T(8,128)(2,1)}, u32[]{:S(2)}) %copy-start.1) | copy-done | bytes 8388632
  7.4 1.2 %copy-done.6 = bf16[2048,256]{1,0:T(8,128)(2,1)S(1)} copy-done((bf16[2048,256]{1,0:T(8,128)(2,1)S(1)}, bf16[2048,256]{1,0:T(8,128)(2,1)}, u32[]{:S(2)}) %copy-start.6) | copy-done | bytes 1048600
  8.7 0.9 %copy-done.7 = bf16[32,2048]{1,0:T(8,128)(2,1)S(1)} copy-done((bf16[32,2048]{1,0:T(8,128)(2,1)S(1)}, bf16[32,2048]{1,0:T(8,128)(2,1)}, u32[]{:S(2)}) %copy-start.7) | copy-done | bytes 131096
  9.6 0.7 copy-done.13
  10.3 0.7 copy-done.15
  10.9 0.7 copy-done.16
  11.6 15.1 %attention.1 = (bf16[32,256]{1,0:T(8,128)(2,1)S(1)}, bf16[256,768]{1,0:T(8,128)(2,1)S(1)}) custom-call(s32[32]{0:T(128)S(1)} %copy-done.15, s32[1]{0:T(128)} %bitcast.place_ref, f32[4]{0:T(128)S(1)} %copy-done.16, bf16[32,2048]{1,0:T(8,128)(2,1)S(1)} %copy-done.7, f32[1,2048]{1,0:T(1,128)S(1)} %bitcast.20, bf16[2048,256]{1,0:T(8,128)(2,1)S(1)} %copy-done.6, ...), custom_call_target="tpu_custom_call" | custom-call | flops 134217728 | bytes 8388608 | tf_op jit(solution)/shard_map/attention/pallas_call | solution.py:285
  26.7 0.7 copy-done.12
  27.5 7.3 %all-to-all-start = ((bf16[32,8,768]{2,1,0:T(8,128)(2,1)}), bf16[32,8,768]{2,1,0:T(8,128)(2,1)S(1)}, u32[]{:S(2)}, u32[]{:S(2)}) async-start(bf16[32,8,768]{2,1,0:T(8,128)(2,1)} %bitcast.18), calls=%async_computation | async-start | bytes 786432 | tf_op jit(solution)/shard_map/all_to_all | solution.py:331
  34.8 5.4 %all-gather = bf16[128,256]{1,0:T(8,128)(2,1)S(1)} all-gather(bf16[32,256]{1,0:T(8,128)(2,1)S(1)} %get-tuple-element.11), channel_id=2, replica_groups=mesh['ep'=8,'tp'=4] {'tp'}, dimensions={0}, use_global_device_ids=true | all-gather | bytes 81920 | tf_op jit(solution)/shard_map/all_gather | solution.py:332
  40.2 7.9 %all-to-all-done = bf16[32,8,768]{2,1,0:T(8,128)(2,1)S(1)} async-done(((bf16[32,8,768]{2,1,0:T(8,128)(2,1)}), bf16[32,8,768]{2,1,0:T(8,128)(2,1)S(1)}, u32[]{:S(2)}, u32[]{:S(2)}) %all-to-all-start) | async-done | bytes 393248 | tf_op jit(solution)/shard_map/all_to_all | solution.py:331
  48.1 2.2 %copy-done.2 = bf16[1024,2048]{1,0:T(8,128)(2,1)S(1)} copy-done((bf16[1024,2048]{1,0:T(8,128)(2,1)S(1)}, bf16[1024,2048]{1,0:T(8,128)(2,1)}, u32[]{:S(2)}) %copy-start.2) | copy-done | bytes 4194328
  50.2 1.6 %copy-done.4 = bf16[1,2048,512]{2,1,0:T(8,128)(2,1)S(1)} copy-done((bf16[1,2048,512]{2,1,0:T(8,128)(2,1)S(1)}, bf16[1,2048,512]{2,1,0:T(8,128)(2,1)}, u32[]{:S(2)}) %copy-start.4) | copy-done | bytes 2097176
  51.8 1.6 %copy-done.5 = bf16[1,512,2048]{2,1,0:T(8,128)(2,1)S(1)} copy-done((bf16[1,512,2048]{2,1,0:T(8,128)(2,1)S(1)}, bf16[1,512,2048]{2,1,0:T(8,128)(2,1)}, u32[]{:S(2)}) %copy-start.5) | copy-done | bytes 2097176
  53.4 3.0 %experts.1 = (bf16[256,512]{1,0:T(8,128)(2,1)}, bf16[32,2048]{1,0:T(8,128)(2,1)S(1)}, bf16[32,2048]{1,0:T(8,128)(2,1)S(1)}) custom-call(bf16[8,32,768]{2,1,0:T(8,128)(2,1)S(1)} %bitcast.16, bf16[4,32,256]{2,1,0:T(8,128)(2,1)S(1)} %bitcast.19, bf16[32,2048]{1,0:T(8,128)(2,1)S(1)} %copy-done.8, bf16[1024,2048]{1,0:T(8,128)(2,1)S(1)} %copy-done.2, ...), custom_call_target="tpu_custom_call" | custom-call | flops 2013265920 | bytes 10485760 | tf_op jit(solution)/shard_map/experts/pallas_call | solution.py:341
  56.4 0.4 shared.1
  56.9 7.0 %all_to_all.25.part_ref = bf16[4,32,512]{2,1,0:T(8,128)(2,1)S(1)} all-to-all(bf16[4,32,512]{2,1,0:T(8,128)(2,1)S(1)} %shared.1), channel_id=1, replica_groups=mesh['ep'=8,'tp'=4] {'tp'}, dimensions={0} | all-to-all | bytes 262144 | tf_op jit(solution)/shard_map/all_to_all | solution.py:382
  63.9 2.6 %all-to-all-start.2 = ((bf16[32,8,512]{2,1,0:T(8,128)(2,1)}), bf16[32,8,512]{2,1,0:T(8,128)(2,1)S(1)}, u32[]{:S(2)}, u32[]{:S(2)}) async-start(bf16[32,8,512]{2,1,0:T(8,128)(2,1)} %bitcast.10), calls=%async_computation.2 | async-start | bytes 524288 | tf_op jit(solution)/shard_map/all_to_all | solution.py:369
  66.5 10.5 %all-to-all-done.2 = bf16[32,8,512]{2,1,0:T(8,128)(2,1)S(1)} async-done(((bf16[32,8,512]{2,1,0:T(8,128)(2,1)}), bf16[32,8,512]{2,1,0:T(8,128)(2,1)S(1)}, u32[]{:S(2)}, u32[]{:S(2)}) %all-to-all-start.2) | async-done | bytes 262176 | tf_op jit(solution)/shard_map/all_to_all | solution.py:369
  77.0 1.1 %combine.1 = bf16[32,512]{1,0:T(8,128)(2,1)} custom-call(s32[1]{0:T(128)} %bitcast.place_ref, bf16[32,2048]{1,0:T(8,128)(2,1)S(1)} %get-tuple-element.12.residual_ref, bf16[4,32,512]{2,1,0:T(8,128)(2,1)S(1)} %all_to_all.25.part_ref, bf16[256,512]{1,0:T(8,128)(2,1)S(1)} %bitcast.17, s32[32,4]{1,0:T(8,128)S(1)} %copy.24.routing_ref, f32[32,4]{1,0:T(8,128)S(1)} %copy.23.rates_ref), custom_call_target="tpu_custom_call" | custom-call | tf_op jit(solution)/shard_map/combine/pallas_call | solution.py:384
  (28 shorter events, 0.3 us)
Async XLA Ops:
  0.0 0.7 copy-start
  4.0 3.4 %copy-start.1 = (bf16[32,1024,128]{2,1,0:T(8,128)(2,1)S(1)}, bf16[32,1024,128]{2,1,0:T(8,128)(2,1)}, u32[]{:S(2)}) copy-start(bf16[32,1024,128]{2,1,0:T(8,128)(2,1)} %kv_ref.1) | copy-start | bytes 25165828
  7.4 1.2 %copy-start.6 = (bf16[2048,256]{1,0:T(8,128)(2,1)S(1)}, bf16[2048,256]{1,0:T(8,128)(2,1)}, u32[]{:S(2)}) copy-start(bf16[2048,256]{1,0:T(8,128)(2,1)} %w_query_ref.1) | copy-start | bytes 3145732
  8.7 0.9 %copy-start.7 = (bf16[32,2048]{1,0:T(8,128)(2,1)S(1)}, bf16[32,2048]{1,0:T(8,128)(2,1)}, u32[]{:S(2)}) copy-start(bf16[32,2048]{1,0:T(8,128)(2,1)} %tokens_ref.3) | copy-start | bytes 393220
  9.6 0.7 copy-start.13
  10.3 0.7 copy-start.15
  10.9 0.7 copy-start.16
  11.6 36.5 %copy-start.3 = (bf16[1,2048,512]{2,1,0:T(8,128)(2,1)S(1)}, bf16[1,2048,512]{2,1,0:T(8,128)(2,1)}, u32[]{:S(2)}) copy-start(bf16[1,2048,512]{2,1,0:T(8,128)(2,1)} %param.35) | copy-start | bytes 6291460
  11.6 36.5 %copy-start.8 = (bf16[32,2048]{1,0:T(8,128)(2,1)S(1)}, bf16[32,2048]{1,0:T(8,128)(2,1)}, u32[]{:S(2)}) copy-start(bf16[32,2048]{1,0:T(8,128)(2,1)} %tokens_ref.3) | copy-start | bytes 393220
  11.6 36.5 %copy-start.14 = (f32[2048]{0:T(1024)S(1)}, f32[2048]{0:T(1024)}, u32[]{:S(2)}) copy-start(f32[2048]{0:T(1024)} %param.29) | copy-start | bytes 24580
  26.7 0.7 copy-start.12
  27.5 20.6 %all-to-all-start = ((bf16[32,8,768]{2,1,0:T(8,128)(2,1)}), bf16[32,8,768]{2,1,0:T(8,128)(2,1)S(1)}, u32[]{:S(2)}, u32[]{:S(2)}) async-start(bf16[32,8,768]{2,1,0:T(8,128)(2,1)} %bitcast.18), calls=%async_computation | async-start | bytes 786432 | tf_op jit(solution)/shard_map/all_to_all | solution.py:331
  48.1 2.2 %copy-start.2 = (bf16[1024,2048]{1,0:T(8,128)(2,1)S(1)}, bf16[1024,2048]{1,0:T(8,128)(2,1)}, u32[]{:S(2)}) copy-start(bf16[1024,2048]{1,0:T(8,128)(2,1)} %w_out_ref.1) | copy-start | bytes 12582916
  50.2 1.6 %copy-start.4 = (bf16[1,2048,512]{2,1,0:T(8,128)(2,1)S(1)}, bf16[1,2048,512]{2,1,0:T(8,128)(2,1)}, u32[]{:S(2)}) copy-start(bf16[1,2048,512]{2,1,0:T(8,128)(2,1)} %param.36) | copy-start | bytes 6291460
  51.8 1.6 %copy-start.5 = (bf16[1,512,2048]{2,1,0:T(8,128)(2,1)S(1)}, bf16[1,512,2048]{2,1,0:T(8,128)(2,1)}, u32[]{:S(2)}) copy-start(bf16[1,512,2048]{2,1,0:T(8,128)(2,1)} %param.37) | copy-start | bytes 6291460
  53.4 3.0 %copy-start.9 = (bf16[2048,128]{1,0:T(8,128)(2,1)S(1)}, bf16[2048,128]{1,0:T(8,128)(2,1)}, u32[]{:S(2)}) copy-start(bf16[2048,128]{1,0:T(8,128)(2,1)} %w_gate_ref.1) | copy-start | bytes 1572868
  53.4 3.0 %copy-start.10 = (bf16[2048,128]{1,0:T(8,128)(2,1)S(1)}, bf16[2048,128]{1,0:T(8,128)(2,1)}, u32[]{:S(2)}) copy-start(bf16[2048,128]{1,0:T(8,128)(2,1)} %w_up_ref.1) | copy-start | bytes 1572868
  53.4 3.0 %copy-start.11 = (bf16[128,2048]{1,0:T(8,128)(2,1)S(1)}, bf16[128,2048]{1,0:T(8,128)(2,1)}, u32[]{:S(2)}) copy-start(bf16[128,2048]{1,0:T(8,128)(2,1)} %w_down_ref.1) | copy-start | bytes 1572868
  56.4 10.0 %copy-start.17 = (f32[32,4]{0,1:T(4,128)S(1)}, f32[32,4]{0,1:T(4,128)}, u32[]{:S(2)}) copy-start(f32[32,4]{0,1:T(4,128)} %param.34) | copy-start | bytes 1540
  63.9 13.2 %all-to-all-start.2 = ((bf16[32,8,512]{2,1,0:T(8,128)(2,1)}), bf16[32,8,512]{2,1,0:T(8,128)(2,1)S(1)}, u32[]{:S(2)}, u32[]{:S(2)}) async-start(bf16[32,8,512]{2,1,0:T(8,128)(2,1)} %bitcast.10), calls=%async_computation.2 | async-start | bytes 524288 | tf_op jit(solution)/shard_map/all_to_all | solution.py:369

commit v2 on v1

v2 whole, which is shorter than its diff:
```python
import functools

import jax
import jax.numpy as jnp
from jax import lax
from jax.experimental import pallas as pl
from jax.experimental.pallas import tpu as pltpu
from jax.sharding import PartitionSpec as P


epsilon = 1e-06
neg_fill = -1e30
f32 = jnp.float32
bf16 = jnp.bfloat16
VMEM = pl.BlockSpec(memory_space=pltpu.VMEM)
SMEM = pl.BlockSpec(memory_space=pltpu.SMEM)
HBM = pl.BlockSpec(memory_space=pltpu.HBM)


def iota(shape, axis):
    return lax.broadcasted_iota(jnp.int32, shape, axis)


def dot(a, b):
    return jnp.dot(a, b, preferred_element_type=f32)


def dot_nt(a, b):
    return lax.dot_general(a, b, (((1,), (1,)), ((), ())), preferred_element_type=f32)


def inv_rms(values):
    return lax.rsqrt(jnp.mean(values * values, axis=-1, keepdims=True) + epsilon)


def slots_of(routing, experts, capacity):
    rows, top_count = routing.shape
    ids = iota((rows, experts), 1)
    hits = [routing[:, k : k + 1] == ids for k in range(top_count)]
    present = jnp.zeros((rows, experts), f32)
    for hit in hits:
        present = jnp.where(hit, 1.0, present)
    earlier = (iota((rows, rows), 1) < iota((rows, rows), 0)).astype(bf16)
    before = dot(earlier, present.astype(bf16))
    ranks = [jnp.sum(jnp.where(hit, before, 0.0), axis=1, keepdims=True) for hit in hits]
    return [
        routing[:, k : k + 1] * capacity + ranks[k].astype(jnp.int32) for k in range(top_count)
    ]


def own_slots(routing_ref, slot_scr, seqs, experts, capacity):
    top_count, batch = routing_ref.shape
    pad = jnp.zeros((8 - top_count, batch), f32)
    slot_scr[...] = jnp.concatenate([routing_ref[...].astype(f32), pad], axis=0).T
    start = pl.multiple_of(lax.axis_index("ep") * seqs, seqs)
    own = slot_scr[pl.ds(start, seqs), :top_count].astype(jnp.int32)
    return slots_of(own, experts, capacity)


def attention_kernel(
    capacity,
    experts,
    block,
    tokens_hbm,
    attn_gain_hbm,
    w_query_hbm,
    w_key_hbm,
    w_value_hbm,
    head_gain_hbm,
    routing_hbm,
    lengths_hbm,
    lambdas_hbm,
    kv_hbm,
    heads_ref,
    send_ref,
    tokens_ref,
    attn_gain_ref,
    w_query_ref,
    w_key_ref,
    w_value_ref,
    head_gain_ref,
    routing_ref,
    lengths_ref,
    lambdas_ref,
    kv_ref,
    q_scr,
    k_scr,
    v_scr,
    o_scr,
    slot_scr,
    sems,
    kv_sems,
):
    seqs, rows, lanes = q_scr.shape
    heads = rows // 2
    v_width = lanes // 2
    qk_width = v_width // 2
    cache_len = kv_ref.shape[1]
    scaling = qk_width ** (-0.5)
    copies = [
        pltpu.make_async_copy(source, target, sems.at[i])
        for i, (source, target) in enumerate(
            [
                (tokens_hbm, tokens_ref),
                (attn_gain_hbm, attn_gain_ref),
                (w_query_hbm, w_query_ref),
                (w_key_hbm, w_key_ref),
                (w_value_hbm, w_value_ref),
                (lengths_hbm, lengths_ref),
                (lambdas_hbm, lambdas_ref),
                (head_gain_hbm, head_gain_ref),
                (routing_hbm, routing_ref),
            ]
        )
    ]
    for copy in copies:
        copy.start()
    steps = seqs // block
    streams = [
        pltpu.make_async_copy(
            kv_hbm.at[pl.ds(i * block, block)], kv_ref.at[pl.ds(i * block, block)], kv_sems.at[i]
        )
        for i in range(steps)
    ]
    for stream in streams[:2]:
        stream.start()
    for copy in copies[:5]:
        copy.wait()
    for stream in streams[2:]:
        stream.start()
    for copy in copies[5:]:
        copy.wait()

    tokens = tokens_ref[...].astype(f32)
    normed = (tokens * inv_rms(tokens) * attn_gain_ref[...]).astype(bf16)
    queries = dot(normed, w_query_ref[...]).astype(bf16).astype(f32)
    pad = jnp.zeros((seqs, v_width), f32)
    k_scr[...] = jnp.concatenate(
        [dot_nt(normed, w_key_ref[...]).astype(bf16).astype(f32), pad], axis=1
    )
    v_scr[...] = jnp.concatenate(
        [pad, dot_nt(normed, w_value_ref[...]).astype(bf16).astype(f32)], axis=1
    )
    lane = iota((seqs, lanes), 1)
    for h in range(heads):
        pair = queries[:, (h // 2) * lanes : (h // 2 + 1) * lanes]
        if h % 2:
            pair = pltpu.roll(pair, v_width, 1)
        for m in range(2):
            keep = (lane >= m * qk_width) & (lane < (m + 1) * qk_width)
            q_scr[:, m * heads + h, :] = jnp.where(keep, pair, 0.0)

    row = iota((rows, 1), 0)
    sign = jnp.where(row < heads, 1.0, 0.0)
    for h in range(heads):
        sign = jnp.where(row == heads + h, -lambdas_ref[h], sign)
    position = iota((rows, cache_len), 1)

    def scores_of(step):
        found = []
        for s in range(step * block, (step + 1) * block):
            found.append(dot_nt(q_scr[s].astype(bf16), kv_ref[s]))
        return found

    def finish(step, found):
        for b in range(block):
            s = step * block + b
            scores = jnp.where(position < lengths_ref[s], found[b] * scaling, neg_fill)
            fresh = jnp.sum(q_scr[s] * k_scr[s : s + 1, :], axis=1, keepdims=True) * scaling
            top = jnp.maximum(jnp.max(scores, axis=1, keepdims=True), fresh)
            expo = jnp.exp(scores - top)
            expo_new = jnp.exp(fresh - top)
            factor = sign / (jnp.sum(expo, axis=1, keepdims=True) + expo_new)
            part = expo * factor
            weights = (part + pltpu.roll(part, heads, 0)).astype(bf16)
            part_new = jnp.broadcast_to(expo_new * factor, (rows, lanes))
            weight_new = (part_new + pltpu.roll(part_new, heads, 0)).astype(bf16).astype(f32)
            o_scr[s] = dot(weights, kv_ref[s]) + weight_new * v_scr[s : s + 1, :]

    held = None
    for step in range(steps):
        streams[step].wait()
        found = scores_of(step)
        if held is not None:
            finish(step - 1, held)
        held = found
    finish(steps - 1, held)

    outs = []
    for h in range(heads):
        mix = jnp.where(lane >= v_width, o_scr[:, h, :], 0.0)
        mean = jnp.sum(mix * mix, axis=1, keepdims=True) * (1.0 / v_width)
        outs.append(mix * lax.rsqrt(mean + epsilon))
    gains = jnp.concatenate([head_gain_ref[...], head_gain_ref[...]], axis=1)
    pairs = [
        jnp.where(lane < v_width, pltpu.roll(outs[2 * p], v_width, 1), outs[2 * p + 1]) * gains
        for p in range(heads // 2)
    ]
    head_out = jnp.concatenate(pairs, axis=1).astype(bf16)
    heads_ref[...] = head_out
    slots = own_slots(routing_ref, slot_scr, seqs, experts, capacity)
    ids = iota((seqs, experts * capacity), 1)
    picks = jnp.zeros((seqs, experts * capacity), f32)
    for slot in slots:
        picks = jnp.where(slot == ids, 1.0, picks)
    picks = picks.T.astype(bf16)
    width = head_out.shape[1]
    share = send_ref.shape[1] - width
    send_ref[:, :width] = dot(picks, head_out).astype(bf16)
    start = pl.multiple_of(lax.axis_index("tp") * share, share)
    send_ref[:, width:] = dot(picks, tokens_ref[:, pl.ds(start, share)]).astype(bf16)


def silu(values):
    return values / (1.0 + jnp.exp(-values))


def partner(index, d, count):
    return index ^ d if count & (count - 1) == 0 else (index + d) % count


def own_kernel(
    capacity,
    experts,
    kept,
    heads_ref,
    w_out_hbm,
    tokens_hbm,
    gain_hbm,
    s_gate_hbm,
    s_up_hbm,
    s_down_hbm,
    routing_hbm,
    rates_hbm,
    *refs,
):
    tp_count, seqs, width = heads_ref.shape
    part_refs = refs[: tp_count - 1]
    base_ref, mix_ref, gain_ref, *kept_refs = refs[tp_count - 1 : tp_count + 2 + kept]
    refs = refs[tp_count + 2 + kept :]
    (
        tokens_ref,
        rest_ref,
        s_gate_ref,
        s_up_ref,
        s_down_ref,
        routing_ref,
        rates_ref,
        res_scr,
        slot_scr,
        sems,
    ) = refs
    share = base_ref.shape[1]
    blocks = column_blocks(w_out_hbm, rest_ref, kept_refs)
    early = [
        (tokens_hbm, tokens_ref),
        (gain_hbm, gain_ref),
        (routing_hbm, routing_ref),
        (rates_hbm, rates_ref),
        *blocks,
        (s_gate_hbm, s_gate_ref),
        (s_up_hbm, s_up_ref),
        (s_down_hbm, s_down_ref),
    ]
    copies = [
        pltpu.make_async_copy(source, target, sems.at[i])
        for i, (source, target) in enumerate(early)
    ]
    for copy in copies:
        copy.start()
    for copy in copies[:4]:
        copy.wait()
    slots = own_slots(routing_ref, slot_scr, seqs, experts, capacity)
    top_count = rates_ref.shape[0]
    rates = jnp.concatenate([rates_ref[...], jnp.zeros((8 - top_count, seqs), f32)], axis=0)
    rates = jnp.concatenate([rates, jnp.zeros((8, 128 - seqs), f32)], axis=1).T[:seqs]
    ids = iota((seqs, experts * capacity), 1)
    mixing = jnp.zeros((seqs, experts * capacity), f32)
    for k, slot in enumerate(slots):
        mixing = jnp.where(slot == ids, rates[:, k : k + 1], mixing)
    high = mixing.astype(bf16)
    mix_ref[:seqs] = high
    mix_ref[seqs:] = (mixing - high.astype(f32)).astype(bf16)

    square = jnp.zeros((seqs, 1), f32)
    for n in range(tp_count):
        copies[4 + n].wait()
        w_out_ref = blocks[n][1]
        cut = slice(n * share, (n + 1) * share)
        total = tokens_ref[:, cut].astype(f32)
        parts = jnp.zeros((seqs, share), f32)
        for j in range(tp_count):
            part = dot(heads_ref[j], w_out_ref[j * width : (j + 1) * width])
            parts = parts + part.astype(bf16).astype(f32)
        residual = (total + parts).astype(bf16).astype(f32)
        res_scr[:, cut] = residual
        square = square + jnp.sum(residual * residual, axis=1, keepdims=True)
    scale = lax.rsqrt(square * (1.0 / res_scr.shape[1]) + epsilon)
    ffn_in = (res_scr[...] * scale * gain_ref[...]).astype(bf16)
    for copy in copies[4 + tp_count :]:
        copy.wait()
    act = silu(dot(ffn_in, s_gate_ref[...])) * dot(ffn_in, s_up_ref[...])
    act = act.astype(bf16)
    for d in range(tp_count):
        start = pl.multiple_of(partner(lax.axis_index("tp"), d, tp_count) * share, share)
        part = dot(act, s_down_ref[:, pl.ds(start, share)])
        if d:
            part_refs[d - 1][...] = part.astype(bf16)
        else:
            base_ref[...] = res_scr[:, pl.ds(start, share)] + part


def column_blocks(w_out_hbm, rest_ref, kept_refs):
    share = rest_ref.shape[2]
    targets = [*kept_refs, *[rest_ref.at[i] for i in range(rest_ref.shape[0])]]
    return [
        (w_out_hbm.at[:, pl.ds(n * share, share)], target) for n, target in enumerate(targets)
    ]


def expert_kernel(
    direct,
    kept,
    arrived_ref,
    gain_ref,
    *refs,
):
    kept_refs = refs[:kept]
    (
        w_out_hbm,
        gate_hbm,
        up_hbm,
        down_hbm,
        send_hbm,
        send_ref,
        rest_ref,
        gate_ref,
        up_ref,
        down_ref,
        res_scr,
        sems,
    ) = refs[kept:]
    blocks = column_blocks(w_out_hbm, rest_ref, kept_refs)
    copies = [
        pltpu.make_async_copy(source, target, sems.at[i])
        for i, (source, target) in enumerate(
            [*blocks[kept:], (gate_hbm, gate_ref), (up_hbm, up_ref), (down_hbm, down_ref)]
        )
    ]
    for copy in copies:
        copy.start()
    groups, chunk, packed = arrived_ref.shape
    rows, model = res_scr.shape
    capacity = rows // groups
    tp_count = chunk // capacity
    share = model // tp_count
    width = packed - share
    lefts = []
    tokens = []
    for j in range(tp_count):
        piece = arrived_ref[:, j * capacity : (j + 1) * capacity, :].astype(f32)
        piece = piece.reshape(rows, packed)
        lefts.append(piece[:, :width].astype(bf16))
        tokens.append(piece[:, width:])
    square = jnp.zeros((rows, 1), f32)
    for n in range(tp_count):
        if n >= kept:
            copies[n - kept].wait()
        w_out_ref = blocks[n][1]
        cut = slice(n * share, (n + 1) * share)
        total = jnp.zeros((rows, share), f32)
        for j in range(tp_count):
            part = dot(lefts[j], w_out_ref[j * width : (j + 1) * width])
            total = total + part.astype(bf16).astype(f32)
        residual = (tokens[n] + total).astype(bf16).astype(f32)
        res_scr[:, cut] = residual
        square = square + jnp.sum(residual * residual, axis=1, keepdims=True)
    scale = lax.rsqrt(square * (1.0 / model) + epsilon)
    ffn_in = (res_scr[...] * scale * gain_ref[...]).astype(bf16)
    copies[-3].wait()
    gate = dot(ffn_in, gate_ref[...])
    copies[-2].wait()
    act = (silu(gate) * dot(ffn_in, up_ref[...])).astype(bf16)
    copies[-1].wait()
    for n in range(tp_count):
        result = dot(act, down_ref[:, n * share : (n + 1) * share])
        if direct:
            for i in range(groups):
                first = (i * tp_count + n) * capacity
                send_ref[first : first + capacity, :] = result[
                    i * capacity : (i + 1) * capacity
                ].astype(bf16)
        else:
            send_ref[:, n * share : (n + 1) * share] = result.astype(bf16)
    back = pltpu.make_async_copy(send_ref, send_hbm, sems.at[0])
    back.start()
    back.wait()


def combine_kernel(base_ref, mix_ref, returned_ref, *refs):
    *part_refs, out_ref = refs
    seqs = out_ref.shape[0]
    returned = returned_ref[...]
    routed = dot(mix_ref[...], returned)
    shared = base_ref[...]
    for part_ref in part_refs:
        shared = shared + part_ref[...].astype(f32)
    out_ref[...] = (shared + routed[:seqs] + routed[seqs:]).astype(bf16)


def params(mib, **more):
    return pltpu.CompilerParams(vmem_limit_bytes=mib << 20, **more)


def shards(
    tokens,
    kv_cache,
    lengths,
    attn_gain,
    w_query,
    w_key,
    w_value,
    lambdas,
    head_gain,
    w_out,
    ffn_gain,
    w_shared_gate,
    w_shared_up,
    w_shared_down,
    routing,
    route_weights,
    w_exp_gate,
    w_exp_up,
    w_exp_down,
):
    seqs, width = tokens.shape
    tp_count = lax.axis_size("tp")
    ep_count = lax.axis_size("ep")
    devices = ep_count * tp_count
    top_count = routing.shape[1]
    experts = w_exp_gate.shape[0] * devices
    capacity = max(2, 2 * seqs * top_count // experts)
    cache_len, lanes = kv_cache.shape[1:]
    v_width = head_gain.shape[0]
    heads = lambdas.shape[0]
    share = width // tp_count
    local = heads * v_width
    packed = local + share
    direct = capacity % 8 == 0
    block = 4
    head_out, send = pl.pallas_call(
        functools.partial(attention_kernel, capacity, experts, block),
        in_specs=[HBM] * 10,
        out_specs=[VMEM] * 2,
        out_shape=[
            pltpu.VMEM((seqs, local), bf16),
            jax.ShapeDtypeStruct((devices * capacity, packed), bf16),
        ],
        scratch_shapes=[
            pltpu.VMEM(tokens.shape, bf16),
            pltpu.VMEM((1, width), f32),
            pltpu.VMEM(w_query.shape, bf16),
            pltpu.VMEM(w_key.shape[::-1], bf16),
            pltpu.VMEM(w_value.shape[::-1], bf16),
            pltpu.VMEM((1, v_width), f32),
            pltpu.VMEM(routing.shape[::-1], jnp.int32),
            pltpu.SMEM(lengths.shape, jnp.int32),
            pltpu.SMEM(lambdas.shape, f32),
            pltpu.VMEM(kv_cache.shape, bf16),
            pltpu.VMEM((seqs, 2 * heads, lanes), f32),
            pltpu.VMEM((seqs, lanes), f32),
            pltpu.VMEM((seqs, lanes), f32),
            pltpu.VMEM((seqs, 2 * heads, lanes), f32),
            pltpu.VMEM((routing.shape[0], 8), f32),
            pltpu.SemaphoreType.DMA((9,)),
            pltpu.SemaphoreType.DMA((seqs // block,)),
        ],
        compiler_params=pltpu.CompilerParams(vmem_limit_bytes=67_043_328 - 2 * seqs * local),
        cost_estimate=pl.CostEstimate(
            flops=seqs * cache_len * lanes * 32, bytes_accessed=kv_cache.size * 2, transcendentals=0
        ),
        name="attention",
    )(
        tokens,
        attn_gain.reshape(1, width),
        w_query,
        w_key.T,
        w_value.T,
        head_gain.reshape(1, v_width),
        routing.T,
        lengths,
        lambdas,
        kv_cache,
    )

    arrived = lax.all_to_all(send, ("ep", "tp"), split_axis=0, concat_axis=0, tiled=True)
    arrived = arrived.reshape(ep_count, tp_count * capacity, packed)
    all_heads = lax.all_gather(head_out, "tp", axis=0, tiled=False)

    exp_gate = w_exp_gate.reshape(w_exp_gate.shape[1:])
    exp_up = w_exp_up.reshape(w_exp_up.shape[1:])
    exp_down = w_exp_down.reshape(w_exp_down.shape[1:])
    rows = ep_count * capacity
    slot_count = experts * capacity
    kept = 1
    w_out_block = (w_out.shape[0], share)
    rest = pltpu.VMEM((tp_count - kept, *w_out_block), bf16)
    results = pl.pallas_call(
        functools.partial(own_kernel, capacity, experts, kept),
        in_specs=[VMEM] + [HBM] * 8,
        out_specs=[VMEM] * (tp_count + 2 + kept),
        out_shape=[pltpu.VMEM((seqs, share), bf16)] * (tp_count - 1)
        + [
            pltpu.VMEM((seqs, share), f32),
            pltpu.VMEM((2 * seqs, slot_count), bf16),
            pltpu.VMEM((1, width), f32),
        ]
        + [pltpu.VMEM(w_out_block, bf16)] * kept,
        scratch_shapes=[
            pltpu.VMEM(tokens.shape, bf16),
            rest,
            pltpu.VMEM(w_shared_gate.shape, bf16),
            pltpu.VMEM(w_shared_up.shape, bf16),
            pltpu.VMEM(w_shared_down.shape, bf16),
            pltpu.VMEM(routing.shape[::-1], jnp.int32),
            pltpu.VMEM(route_weights.shape[::-1], f32),
            pltpu.VMEM((seqs, width), f32),
            pltpu.VMEM((routing.shape[0], 8), f32),
            pltpu.SemaphoreType.DMA((7 + tp_count,)),
        ],
        compiler_params=pltpu.CompilerParams(vmem_limit_bytes=63_900_000),
        cost_estimate=pl.CostEstimate(
            flops=2 * seqs * w_out.size, bytes_accessed=12 << 20, transcendentals=0
        ),
        name="own",
    )(
        all_heads,
        w_out,
        tokens,
        ffn_gain.reshape(1, width),
        w_shared_gate,
        w_shared_up,
        w_shared_down,
        routing.T,
        route_weights.T,
    )

    part, (base, mix, gain), kept_blocks = (
        results[: tp_count - 1],
        results[tp_count - 1 : tp_count + 2],
        results[tp_count + 2 :],
    )
    arrived, gain, *kept_blocks = [
        pltpu.with_memory_space_constraint(value, pltpu.VMEM)
        for value in (arrived, gain, *kept_blocks)
    ]
    sent_shape = (devices * capacity, share) if direct else (rows, width)
    sent = pl.pallas_call(
        functools.partial(expert_kernel, direct, kept),
        in_specs=[VMEM] * (2 + kept) + [HBM] * 4,
        out_specs=HBM,
        out_shape=jax.ShapeDtypeStruct(sent_shape, bf16),
        scratch_shapes=[
            pltpu.VMEM(sent_shape, bf16),
            rest,
            pltpu.VMEM(exp_gate.shape, bf16),
            pltpu.VMEM(exp_up.shape, bf16),
            pltpu.VMEM(exp_down.shape, bf16),
            pltpu.VMEM((rows, width), f32),
            pltpu.SemaphoreType.DMA((3 + tp_count - kept,)),
        ],
        compiler_params=pltpu.CompilerParams(vmem_limit_bytes=60 * 1024 * 1024),
        cost_estimate=pl.CostEstimate(
            flops=2 * rows * 5 * w_out.size // 2, bytes_accessed=1 << 20, transcendentals=0
        ),
        name="experts",
    )(arrived, gain, *kept_blocks, w_out, exp_gate, exp_up, exp_down)
    if not direct:
        sent = sent.reshape(ep_count, capacity, tp_count, share)
        sent = sent.transpose(0, 2, 1, 3).reshape(devices * capacity, share)
    returned = lax.all_to_all(sent, ("ep", "tp"), split_axis=0, concat_axis=0, tiled=True)
    parts = [
        lax.ppermute(piece, "tp", [(i, partner(i, d, tp_count)) for i in range(tp_count)])
        for d, piece in enumerate(part, 1)
    ]

    return pl.pallas_call(
        combine_kernel,
        in_specs=[VMEM] * (tp_count + 2),
        out_specs=VMEM,
        out_shape=jax.ShapeDtypeStruct((seqs, share), bf16),
        compiler_params=params(16),
        name="combine",
    )(base, mix, returned, *parts)


def solution(mesh):
    return jax.shard_map(
        shards,
        mesh=mesh,
        in_specs=(
            P("ep", None),
            P("ep", None, "tp"),
            P("ep"),
            P(),
            P(None, "tp"),
            P(None, "tp"),
            P(None, "tp"),
            P("tp"),
            P(),
            P(),
            P(),
            P(None, "tp"),
            P(None, "tp"),
            P("tp", None),
            P(),
            P("ep", None),
            P(("ep", "tp"), None, None),
            P(("ep", "tp"), None, None),
            P(("ep", "tp"), None, None),
        ),
        out_specs=P("ep", "tp"),
        check_vma=False,
    )
```

time: 78.8 us -> 48.7 us (0.62)
  local copies, waits for them, and re-layouts: 17.8 us -> 0 us
  waiting for transfers between devices: 18.3 us -> 11.6 us
  blocking collectives: 12.4 us -> 5.82 us
  starting transfers between devices: 9.91 us -> 12.5 us
  Pallas kernels: 19.7 us -> 18.4 us
    unnamed x40 -> x0, local copies, waits for them, and re-layouts: 17 us -> none
    all_to_all x1 -> x0, blocking collectives: 6.99 us -> none  [shards(): parts = lax.all_to_all(part, 'tp', split_axis=0, concat_axis=0, tiled=True)]
    all_to_all x1, waiting for transfers between devices: 10.5 us -> 4.57 us  [shards(): lax.all_to_all(sent, ('ep', 'tp'), split_axis=0, concat_axis=0, tiled=True)]
    all_to_all x1, waiting for transfers between devices: 7.87 us -> 3 us  [shards(): lax.all_to_all(send, ('ep', 'tp'), split_axis=0, concat_axis=0, tiled=True)]
    ppermute x0 -> x3, waiting for transfers between devices: none -> 4.05 us  [shards(): lax.ppermute(piece, 'tp', [(i, partner(i, d, tp_count)) for i in range(tp...]
    ppermute x0 -> x3, starting transfers between devices: none -> 1.95 us  [shards(): lax.ppermute(piece, 'tp', [(i, partner(i, d, tp_count)) for i in range(tp...]
    pallas_call x4, Pallas kernels: 19.7 us -> 18.4 us  [the longest x1 7.97 us: shards(): pl.pallas_call(functools.partial(attention_kernel, capacity, experts, blo...]
  transfers between devices with their start and end apart: 2 -> 5, of which waited for: 2 -> 4; matrix products, arithmetic and copies ran while one was open for 0% -> 0% of each run, Pallas kernels for 0% -> 9%
where the time goes in v2:
time: 48.7 us; the launch traced here: 48.4 us
  Pallas kernels  18.4 us (38%)
  starting transfers between devices  12.5 us (26%)
  waiting for transfers between devices  11.6 us (24%)
  blocking collectives  5.82 us (12%)
    pallas_call x1, Pallas kernels, shards(): pl.pallas_call(functools.partial(attention_kernel, capacity, experts, blo...  7.97 us
    all_to_all x1, starting transfers between devices, shards(): lax.all_to_all(send, ('ep', 'tp'), split_axis=0, concat_axis=0, tiled=True)  7.34 us
    all_gather x1, blocking collectives, shards(): all_heads = lax.all_gather(head_out, 'tp', axis=0, tiled=False)  5.82 us
    pallas_call x1, Pallas kernels, shards(): pl.pallas_call(functools.partial(expert_kernel, direct, kept), in_specs=[...  5.21 us
    all_to_all x1, waiting for transfers between devices, shards(): lax.all_to_all(sent, ('ep', 'tp'), split_axis=0, concat_axis=0, tiled=True)  4.57 us
    pallas_call x1, Pallas kernels, shards(): pl.pallas_call(functools.partial(own_kernel, capacity, experts, kept), in...  4.42 us
    ppermute x3, waiting for transfers between devices, shards(): lax.ppermute(piece, 'tp', [(i, partner(i, d, tp_count)) for i in range(tp...  4.05 us
    all_to_all x1, starting transfers between devices, shards(): lax.all_to_all(sent, ('ep', 'tp'), split_axis=0, concat_axis=0, tiled=True)  3.24 us
  transfers between devices with their start and end apart: 5, of which 4 were waited for; matrix products, arithmetic and copies ran while one was open for 0% of the time, Pallas kernels for 9%

profile of v2, /device:TPU:0, one launch (start us, length us, event | category | flops | bytes accessed | tf_op | source)
XLA Modules:
  0.0 48.4 jit_solution(12723958669691184839)
XLA Ops:
  0.0 8.0 %attention.1 = (bf16[32,256]{1,0:T(8,128)(2,1)S(1)}, bf16[256,768]{1,0:T(8,128)(2,1)}) custom-call(bf16[32,2048]{1,0:T(8,128)(2,1)} %tokens_hbm.3, f32[1,2048]{1,0:T(1,128)} %bitcast.28, bf16[2048,256]{1,0:T(8,128)(2,1)} %w_query_hbm.1, bf16[64,2048]{1,0:T(8,128)(2,1)} %bitcast.23, bf16[64,2048]{1,0:T(8,128)(2,1)} %bitcast.24, f32[1,64]{1,0:T(1,128)} %bitcast.30, ...), custom_call_target="tpu_custom_call" | custom-call | flops 134217728 | bytes 8388608 | tf_op jit(solution)/shard_map/attention/pallas_call | solution.py:451
  8.0 7.3 %all-to-all-start = ((bf16[32,8,768]{2,1,0:T(8,128)(2,1)}), bf16[32,8,768]{2,1,0:T(8,128)(2,1)S(1)}, u32[]{:S(2)}, u32[]{:S(2)}) async-start(bf16[32,8,768]{2,1,0:T(8,128)(2,1)} %bitcast.21), calls=%async_computation | async-start | bytes 786432 | tf_op jit(solution)/shard_map/all_to_all | solution.py:496
  15.3 5.8 %all-gather = bf16[128,256]{1,0:T(8,128)(2,1)} all-gather(bf16[32,256]{1,0:T(8,128)(2,1)S(1)} %get-tuple-element.14), channel_id=2, replica_groups=mesh['ep'=8,'tp'=4] {'tp'}, dimensions={0}, use_global_device_ids=true | all-gather | bytes 81920 | tf_op jit(solution)/shard_map/all_gather | solution.py:498
  21.2 4.4 %own.1 = (bf16[32,512]{1,0:T(8,128)(2,1)S(1)}, bf16[32,512]{1,0:T(8,128)(2,1)S(1)}, bf16[32,512]{1,0:T(8,128)(2,1)S(1)}, f32[32,512]{1,0:T(8,128)S(1)}, bf16[64,...) custom-call(bf16[4,32,256]{2,1,0:T(8,128)(2,1)} %bitcast.22, ...), custom_call_target="tpu_custom_call" | custom-call | flops 134217728 | bytes 12582912 | tf_op jit(solution)/shard_map/own/pallas_call | solution.py:508
  25.6 3.0 %all-to-all-done = bf16[32,8,768]{2,1,0:T(8,128)(2,1)S(1)} async-done(((bf16[32,8,768]{2,1,0:T(8,128)(2,1)}), bf16[32,8,768]{2,1,0:T(8,128)(2,1)S(1)}, u32[]{:S(2)}, u32[]{:S(2)}) %all-to-all-start) | async-done | bytes 393248 | tf_op jit(solution)/shard_map/all_to_all | solution.py:496
  28.6 5.2 %experts.1 = bf16[256,512]{1,0:T(8,128)(2,1)} custom-call(bf16[8,32,768]{2,1,0:T(8,128)(2,1)S(1)} %bitcast.15, f32[1,2048]{1,0:T(1,128)S(1)} %get-tuple-element.18.gain_ref, bf16[1024,512]{1,0:T(8,128)(2,1)S(1)} %get-tuple-element.19.refs_0_, bf16[1024,2048]{1,0:T(8,128)(2,1)} %refs_1_.1, bf16[2048,512]{1,0:T(8,128)(2,1)} %bitcast.17, ...), custom_call_target="tpu_custom_call" | custom-call | flops 671088640 | bytes 1048576 | tf_op jit(solution)/shard_map/experts/pallas_call | solution.py:558
  33.8 3.2 %all-to-all-start.1 = ((bf16[32,8,512]{2,1,0:T(8,128)(2,1)}), bf16[32,8,512]{2,1,0:T(8,128)(2,1)S(1)}, u32[]{:S(2)}, u32[]{:S(2)}) async-start(bf16[32,8,512]{2,1,0:T(8,128)(2,1)} %bitcast.20), calls=%async_computation.1 | async-start | bytes 524288 | tf_op jit(solution)/shard_map/all_to_all | solution.py:581
  37.0 0.3 collective-permute-start
  37.4 1.6 %collective-permute-start.1 = (bf16[32,512]{1,0:T(8,128)(2,1)S(1)}, bf16[32,512]{1,0:T(8,128)(2,1)S(1)}, u32[]{:S(2)}, u32[]{:S(2)}) collective-permute-start(bf16[32,512]{1,0:T(8,128)(2,1)S(1)} %get-tuple-element.21), channel_id=1, source_target_pairs={{0,2},{1,3},{2,0},{3,1},{4,6},{5,7},{6,4},{7,5},{8,10},{9,11},{10,... | collective-permute-start | bytes 98312 | tf_op jit(solution)/shard_map/ppermute | solution.py:583
  39.0 0.0 collective-permute-start.2
  39.0 0.0 collective-permute-done.refs_0_
  39.0 2.6 %collective-permute-done.1.refs_1_ = bf16[32,512]{1,0:T(8,128)(2,1)S(1)} collective-permute-done((bf16[32,512]{1,0:T(8,128)(2,1)S(1)}, bf16[32,512]{1,0:T(8,128)(2,1)S(1)}, u32[]{:S(2)}, u32[]{:S(2)}) %collective-permute-start.1) | collective-permute-done | bytes 32800 | tf_op jit(solution)/shard_map/ppermute | solution.py:583
  41.6 1.4 %collective-permute-done.2.refs_2_ = bf16[32,512]{1,0:T(8,128)(2,1)S(1)} collective-permute-done((bf16[32,512]{1,0:T(8,128)(2,1)S(1)}, bf16[32,512]{1,0:T(8,128)(2,1)S(1)}, u32[]{:S(2)}, u32[]{:S(2)}) %collective-permute-start.2) | collective-permute-done | bytes 32800 | tf_op jit(solution)/shard_map/ppermute | solution.py:583
  43.0 4.6 %all-to-all-done.1 = bf16[32,8,512]{2,1,0:T(8,128)(2,1)S(1)} async-done(((bf16[32,8,512]{2,1,0:T(8,128)(2,1)}), bf16[32,8,512]{2,1,0:T(8,128)(2,1)S(1)}, u32[]{:S(2)}, u32[]{:S(2)}) %all-to-all-start.1) | async-done | bytes 262176 | tf_op jit(solution)/shard_map/all_to_all | solution.py:581
  47.6 0.8 %combine.1 = bf16[32,512]{1,0:T(8,128)(2,1)} custom-call(f32[32,512]{1,0:T(8,128)S(1)} %get-tuple-element.15.base_ref, bf16[64,256]{1,0:T(8,128)(2,1)S(1)} %get-tuple-element.16.mix_ref, bf16[256,512]{1,0:T(8,128)(2,1)S(1)} %bitcast.16, bf16[32,512]{1,0:T(8,128)(2,1)S(1)} %collective-permute-done.refs_0_, ...), custom_call_target="tpu_custom_call" | custom-call | tf_op jit(solution)/shard_map/combine/pallas_call | solution.py:587
Async XLA Ops:
  8.0 20.6 %all-to-all-start = ((bf16[32,8,768]{2,1,0:T(8,128)(2,1)}), bf16[32,8,768]{2,1,0:T(8,128)(2,1)S(1)}, u32[]{:S(2)}, u32[]{:S(2)}) async-start(bf16[32,8,768]{2,1,0:T(8,128)(2,1)} %bitcast.21), calls=%async_computation | async-start | bytes 786432 | tf_op jit(solution)/shard_map/all_to_all | solution.py:496
  33.8 13.8 %all-to-all-start.1 = ((bf16[32,8,512]{2,1,0:T(8,128)(2,1)}), bf16[32,8,512]{2,1,0:T(8,128)(2,1)S(1)}, u32[]{:S(2)}, u32[]{:S(2)}) async-start(bf16[32,8,512]{2,1,0:T(8,128)(2,1)} %bitcast.20), calls=%async_computation.1 | async-start | bytes 524288 | tf_op jit(solution)/shard_map/all_to_all | solution.py:581
  37.0 2.0 %collective-permute-start = (bf16[32,512]{1,0:T(8,128)(2,1)S(1)}, bf16[32,512]{1,0:T(8,128)(2,1)S(1)}, u32[]{:S(2)}, u32[]{:S(2)}) collective-permute-start(bf16[32,512]{1,0:T(8,128)(2,1)S(1)} %get-tuple-element.20), channel_id=1, source_target_pairs={{0,1},{1,0},{2,3},{3,2},{4,5},{5,4},{6,7},{7,6},{8,9},{9,8},{10,11... | collective-permute-start | bytes 98312 | tf_op jit(solution)/shard_map/ppermute | solution.py:583
  37.4 4.3 %collective-permute-start.1 = (bf16[32,512]{1,0:T(8,128)(2,1)S(1)}, bf16[32,512]{1,0:T(8,128)(2,1)S(1)}, u32[]{:S(2)}, u32[]{:S(2)}) collective-permute-start(bf16[32,512]{1,0:T(8,128)(2,1)S(1)} %get-tuple-element.21), channel_id=1, source_target_pairs={{0,2},{1,3},{2,0},{3,1},{4,6},{5,7},{6,4},{7,5},{8,10},{9,11},{10,... | collective-permute-start | bytes 98312 | tf_op jit(solution)/shard_map/ppermute | solution.py:583
  39.0 4.1 %collective-permute-start.2 = (bf16[32,512]{1,0:T(8,128)(2,1)S(1)}, bf16[32,512]{1,0:T(8,128)(2,1)S(1)}, u32[]{:S(2)}, u32[]{:S(2)}) collective-permute-start(bf16[32,512]{1,0:T(8,128)(2,1)S(1)} %get-tuple-element.22), channel_id=1, source_target_pairs={{0,3},{1,2},{2,1},{3,0},{4,7},{5,6},{6,5},{7,4},{8,11},{9,10},{10,... | collective-permute-start | bytes 98312 | tf_op jit(solution)/shard_map/ppermute | solution.py:583

commit v3 on v2

--- a/solution.py
+++ b/solution.py
@@ -72,7 +72,7 @@
     lambdas_hbm,
     kv_hbm,
     heads_ref,
-    send_ref,
+    send_hbm,
     tokens_ref,
     attn_gain_ref,
     w_query_ref,
@@ -88,14 +88,19 @@
     v_scr,
     o_scr,
     slot_scr,
+    back_scr,
+    mix_scr,
     sems,
     kv_sems,
+    back_sems,
 ):
     seqs, rows, lanes = q_scr.shape
     heads = rows // 2
     v_width = lanes // 2
     qk_width = v_width // 2
     cache_len = kv_ref.shape[1]
+    width = mix_scr.shape[1]
+    share = back_scr.shape[1]
     scaling = qk_width ** (-0.5)
     copies = [
         pltpu.make_async_copy(source, target, sems.at[i])
@@ -103,13 +108,13 @@
             [
                 (tokens_hbm, tokens_ref),
                 (attn_gain_hbm, attn_gain_ref),
+                (routing_hbm, routing_ref),
                 (w_query_hbm, w_query_ref),
                 (w_key_hbm, w_key_ref),
                 (w_value_hbm, w_value_ref),
                 (lengths_hbm, lengths_ref),
                 (lambdas_hbm, lambdas_ref),
                 (head_gain_hbm, head_gain_ref),
-                (routing_hbm, routing_ref),
             ]
         )
     ]
@@ -122,93 +127,112 @@
         )
         for i in range(steps)
     ]
-    for stream in streams[:2]:
+    streams[0].start()
+    for copy in copies[:3]:
+        copy.wait()
+    for stream in streams[1:]:
         stream.start()
-    for copy in copies[:5]:
-        copy.wait()
-    for stream in streams[2:]:
-        stream.start()
-    for copy in copies[5:]:
-        copy.wait()
-
-    tokens = tokens_ref[...].astype(f32)
-    normed = (tokens * inv_rms(tokens) * attn_gain_ref[...]).astype(bf16)
-    queries = dot(normed, w_query_ref[...]).astype(bf16).astype(f32)
-    pad = jnp.zeros((seqs, v_width), f32)
-    k_scr[...] = jnp.concatenate(
-        [dot_nt(normed, w_key_ref[...]).astype(bf16).astype(f32), pad], axis=1
-    )
-    v_scr[...] = jnp.concatenate(
-        [pad, dot_nt(normed, w_value_ref[...]).astype(bf16).astype(f32)], axis=1
-    )
-    lane = iota((seqs, lanes), 1)
-    for h in range(heads):
-        pair = queries[:, (h // 2) * lanes : (h // 2 + 1) * lanes]
-        if h % 2:
-            pair = pltpu.roll(pair, v_width, 1)
-        for m in range(2):
-            keep = (lane >= m * qk_width) & (lane < (m + 1) * qk_width)
-            q_scr[:, m * heads + h, :] = jnp.where(keep, pair, 0.0)
-
-    row = iota((rows, 1), 0)
-    sign = jnp.where(row < heads, 1.0, 0.0)
-    for h in range(heads):
-        sign = jnp.where(row == heads + h, -lambdas_ref[h], sign)
-    position = iota((rows, cache_len), 1)
-
-    def scores_of(step):
-        found = []
-        for s in range(step * block, (step + 1) * block):
-            found.append(dot_nt(q_scr[s].astype(bf16), kv_ref[s]))
-        return found
-
-    def finish(step, found):
-        for b in range(block):
-            s = step * block + b
-            scores = jnp.where(position < lengths_ref[s], found[b] * scaling, neg_fill)
-            fresh = jnp.sum(q_scr[s] * k_scr[s : s + 1, :], axis=1, keepdims=True) * scaling
-            top = jnp.maximum(jnp.max(scores, axis=1, keepdims=True), fresh)
-            expo = jnp.exp(scores - top)
-            expo_new = jnp.exp(fresh - top)
-            factor = sign / (jnp.sum(expo, axis=1, keepdims=True) + expo_new)
-            part = expo * factor
-            weights = (part + pltpu.roll(part, heads, 0)).astype(bf16)
-            part_new = jnp.broadcast_to(expo_new * factor, (rows, lanes))
-            weight_new = (part_new + pltpu.roll(part_new, heads, 0)).astype(bf16).astype(f32)
-            o_scr[s] = dot(weights, kv_ref[s]) + weight_new * v_scr[s : s + 1, :]
-
-    held = None
-    for step in range(steps):
-        streams[step].wait()
-        found = scores_of(step)
-        if held is not None:
-            finish(step - 1, held)
-        held = found
-    finish(steps - 1, held)
-
-    outs = []
-    for h in range(heads):
-        mix = jnp.where(lane >= v_width, o_scr[:, h, :], 0.0)
-        mean = jnp.sum(mix * mix, axis=1, keepdims=True) * (1.0 / v_width)
-        outs.append(mix * lax.rsqrt(mean + epsilon))
-    gains = jnp.concatenate([head_gain_ref[...], head_gain_ref[...]], axis=1)
-    pairs = [
-        jnp.where(lane < v_width, pltpu.roll(outs[2 * p], v_width, 1), outs[2 * p + 1]) * gains
-        for p in range(heads // 2)
-    ]
-    head_out = jnp.concatenate(pairs, axis=1).astype(bf16)
-    heads_ref[...] = head_out
+
     slots = own_slots(routing_ref, slot_scr, seqs, experts, capacity)
     ids = iota((seqs, experts * capacity), 1)
     picks = jnp.zeros((seqs, experts * capacity), f32)
     for slot in slots:
         picks = jnp.where(slot == ids, 1.0, picks)
     picks = picks.T.astype(bf16)
-    width = head_out.shape[1]
-    share = send_ref.shape[1] - width
-    send_ref[:, :width] = dot(picks, head_out).astype(bf16)
     start = pl.multiple_of(lax.axis_index("tp") * share, share)
-    send_ref[:, width:] = dot(picks, tokens_ref[:, pl.ds(start, share)]).astype(bf16)
+    back_scr[...] = dot(picks, tokens_ref[:, pl.ds(start, share)]).astype(bf16)
+    backs = [
+        pltpu.make_async_copy(back_scr, send_hbm.at[:, pl.ds(width, share)], back_sems.at[0]),
+        pltpu.make_async_copy(mix_scr, send_hbm.at[:, pl.ds(0, width)], back_sems.at[1]),
+    ]
+    backs[0].start()
+    tokens = tokens_ref[...].astype(f32)
+    normed = (tokens * inv_rms(tokens) * attn_gain_ref[...]).astype(bf16)
+
+    for copy in copies[3:]:
+        copy.wait()
+    queries = dot(normed, w_query_ref[...]).astype(bf16).astype(f32)
+    key_new = dot_nt(normed, w_key_ref[...]).astype(bf16).astype(f32)
+    value_new = dot_nt(normed, w_value_ref[...]).astype(bf16).astype(f32)
+    k_scr[...] = jnp.concatenate([key_new, key_new], axis=1)
+    v_scr[...] = jnp.concatenate([value_new, value_new], axis=1)
+    lane = iota((seqs, lanes), 1)
+    upper = lane >= v_width
+    own_keys = upper == (iota((seqs, lanes), 0) % 2 == 1)
+    for h in range(heads):
+        pair = queries[:, (h // 2) * lanes : (h // 2 + 1) * lanes]
+        pair = jnp.where(upper == (h % 2 == 1), pair, pltpu.roll(pair, v_width, 1))
+        for m in range(2):
+            inner = lane % v_width
+            keep = own_keys & (inner >= m * qk_width) & (inner < (m + 1) * qk_width)
+            q_scr[:, m * heads + h, :] = jnp.where(keep, pair, 0.0)
+
+    row = iota((2 * rows, 1), 0) % rows
+    sign = jnp.where(row < heads, 1.0, 0.0)
+    for h in range(heads):
+        sign = jnp.where(row == heads + h, -lambdas_ref[h], sign)
+    position = iota((2 * rows, cache_len), 1)
+    second = iota((2 * rows, 1), 0) >= rows
+
+    def scores_of(step):
+        found = []
+        for b in range(0, block, 2):
+            s = step * block + b
+            even, odd = kv_ref[s], kv_ref[s + 1]
+            query = q_scr[s : s + 2].reshape(2 * rows, lanes).astype(bf16)
+            keys = jnp.concatenate([even[:, :v_width], odd[:, :v_width]], axis=1)
+            values = jnp.concatenate([odd[:, v_width:], even[:, v_width:]], axis=1)
+            found.append((dot_nt(query, keys), values))
+        return found
+
+    def fold(part):
+        halves = [part[i * rows : (i + 1) * rows] for i in range(2)]
+        return jnp.concatenate([half + pltpu.roll(half, heads, 0) for half in halves], axis=0)
+
+    def finish(step, found):
+        for b in range(0, block, 2):
+            s = step * block + b
+            length = jnp.where(second, lengths_ref[s + 1], lengths_ref[s])
+            scores = jnp.where(position < length, found[b // 2][0] * scaling, neg_fill)
+            fresh = jnp.sum(q_scr[s : s + 2] * k_scr[s : s + 2][:, None, :], axis=2, keepdims=True)
+            fresh = fresh.reshape(2 * rows, 1) * scaling
+            top = jnp.maximum(jnp.max(scores, axis=1, keepdims=True), fresh)
+            expo = jnp.exp(scores - top)
+            expo_new = jnp.exp(fresh - top)
+            factor = sign / (jnp.sum(expo, axis=1, keepdims=True) + expo_new)
+            part_new = jnp.broadcast_to(expo_new * factor, (2 * rows, lanes))
+            weights = fold(expo * factor).astype(bf16)
+            weight_new = fold(part_new).astype(bf16).astype(f32)
+            mixed = dot(weights, found[b // 2][1]).reshape(2, rows, lanes)
+            o_scr[s : s + 2] = (
+                mixed + weight_new.reshape(2, rows, lanes) * v_scr[s : s + 2][:, None, :]
+            )
+
+    held = None
+    for step in range(steps + 1):
+        if step < steps:
+            streams[step].wait()
+            found = scores_of(step)
+        if step:
+            finish(step - 1, held)
+        held = found
+
+    outs = []
+    for h in range(heads):
+        mix = jnp.where(own_keys, 0.0, o_scr[:, h, :])
+        mean = jnp.sum(mix * mix, axis=1, keepdims=True) * (1.0 / v_width)
+        mix = mix * lax.rsqrt(mean + epsilon)
+        outs.append(mix + pltpu.roll(mix, v_width, 1))
+    gains = jnp.concatenate([head_gain_ref[...], head_gain_ref[...]], axis=1)
+    pairs = [
+        jnp.where(upper, outs[2 * p + 1], outs[2 * p]) * gains for p in range(heads // 2)
+    ]
+    head_out = jnp.concatenate(pairs, axis=1).astype(bf16)
+    heads_ref[...] = head_out
+    mix_scr[...] = dot(picks, head_out).astype(bf16)
+    backs[1].start()
+    for back in backs:
+        back.wait()
 
 
 def silu(values):
@@ -344,7 +368,12 @@
     copies = [
         pltpu.make_async_copy(source, target, sems.at[i])
         for i, (source, target) in enumerate(
-            [*blocks[kept:], (gate_hbm, gate_ref), (up_hbm, up_ref), (down_hbm, down_ref)]
+            [
+                *blocks[kept:],
+                (gate_hbm, gate_ref),
+                (up_hbm, up_ref),
+                *column_blocks(down_hbm, down_ref, ()),
+            ]
         )
     ]
     for copy in copies:
@@ -377,13 +406,13 @@
         square = square + jnp.sum(residual * residual, axis=1, keepdims=True)
     scale = lax.rsqrt(square * (1.0 / model) + epsilon)
     ffn_in = (res_scr[...] * scale * gain_ref[...]).astype(bf16)
-    copies[-3].wait()
+    copies[tp_count - kept].wait()
     gate = dot(ffn_in, gate_ref[...])
-    copies[-2].wait()
+    copies[tp_count - kept + 1].wait()
     act = (silu(gate) * dot(ffn_in, up_ref[...])).astype(bf16)
-    copies[-1].wait()
     for n in range(tp_count):
-        result = dot(act, down_ref[:, n * share : (n + 1) * share])
+        copies[n - tp_count].wait()
+        result = dot(act, down_ref[n])
         if direct:
             for i in range(groups):
                 first = (i * tp_count + n) * capacity
@@ -451,7 +480,7 @@
     head_out, send = pl.pallas_call(
         functools.partial(attention_kernel, capacity, experts, block),
         in_specs=[HBM] * 10,
-        out_specs=[VMEM] * 2,
+        out_specs=[VMEM, HBM],
         out_shape=[
             pltpu.VMEM((seqs, local), bf16),
             jax.ShapeDtypeStruct((devices * capacity, packed), bf16),
@@ -472,8 +501,11 @@
             pltpu.VMEM((seqs, lanes), f32),
             pltpu.VMEM((seqs, 2 * heads, lanes), f32),
             pltpu.VMEM((routing.shape[0], 8), f32),
+            pltpu.VMEM((devices * capacity, share), bf16),
+            pltpu.VMEM((devices * capacity, local), bf16),
             pltpu.SemaphoreType.DMA((9,)),
             pltpu.SemaphoreType.DMA((seqs // block,)),
+            pltpu.SemaphoreType.DMA((2,)),
         ],
         compiler_params=pltpu.CompilerParams(vmem_limit_bytes=67_043_328 - 2 * seqs * local),
         cost_estimate=pl.CostEstimate(
@@ -565,9 +597,9 @@
             rest,
             pltpu.VMEM(exp_gate.shape, bf16),
             pltpu.VMEM(exp_up.shape, bf16),
-            pltpu.VMEM(exp_down.shape, bf16),
+            pltpu.VMEM((tp_count, exp_down.shape[0], share), bf16),
             pltpu.VMEM((rows, width), f32),
-            pltpu.SemaphoreType.DMA((3 + tp_count - kept,)),
+            pltpu.SemaphoreType.DMA((2 + 2 * tp_count - kept,)),
         ],
         compiler_params=pltpu.CompilerParams(vmem_limit_bytes=60 * 1024 * 1024),
         cost_estimate=pl.CostEstimate(

time: 48.7 us -> 48.2 us (0.990)
  Pallas kernels: 18.4 us -> 17.9 us
    pallas_call x1, Pallas kernels: 7.97 us -> 7.34 us  [shards(): pl.pallas_call(functools.partial(attention_kernel, capacity, experts, blo...]
where the time goes in v3:
time: 48.2 us; the launch traced here: 47.9 us
  Pallas kernels  17.9 us (37%)
  starting transfers between devices  12.5 us (26%)
  waiting for transfers between devices  11.6 us (24%)
  blocking collectives  5.82 us (12%)
    all_to_all x1, starting transfers between devices, shards(): lax.all_to_all(send, ('ep', 'tp'), split_axis=0, concat_axis=0, tiled=True)  7.34 us
    pallas_call x1, Pallas kernels, shards(): pl.pallas_call(functools.partial(attention_kernel, capacity, experts, blo...  7.34 us
    all_gather x1, blocking collectives, shards(): all_heads = lax.all_gather(head_out, 'tp', axis=0, tiled=False)  5.82 us
    pallas_call x1, Pallas kernels, shards(): pl.pallas_call(functools.partial(expert_kernel, direct, kept), in_specs=[...  5.32 us
    all_to_all x1, waiting for transfers between devices, shards(): lax.all_to_all(sent, ('ep', 'tp'), split_axis=0, concat_axis=0, tiled=True)  4.57 us
    pallas_call x1, Pallas kernels, shards(): pl.pallas_call(functools.partial(own_kernel, capacity, experts, kept), in...  4.42 us
    ppermute x3, waiting for transfers between devices, shards(): lax.ppermute(piece, 'tp', [(i, partner(i, d, tp_count)) for i in range(tp...  4.05 us
    all_to_all x1, starting transfers between devices, shards(): lax.all_to_all(sent, ('ep', 'tp'), split_axis=0, concat_axis=0, tiled=True)  3.25 us
  transfers between devices with their start and end apart: 5, of which 4 were waited for; matrix products, arithmetic and copies ran while one was open for 0% of the time, Pallas kernels for 9%

profile of v3, /device:TPU:0, one launch (start us, length us, event | category | flops | bytes accessed | tf_op | source)
XLA Modules:
  0.0 47.9 jit_solution(625598345538186044)
XLA Ops:
  0.0 7.3 %attention.1 = (bf16[32,256]{1,0:T(8,128)(2,1)S(1)}, bf16[256,768]{1,0:T(8,128)(2,1)}) custom-call(bf16[32,2048]{1,0:T(8,128)(2,1)} %tokens_hbm.3, f32[1,2048]{1,0:T(1,128)} %bitcast.28, bf16[2048,256]{1,0:T(8,128)(2,1)} %w_query_hbm.1, bf16[64,2048]{1,0:T(8,128)(2,1)} %bitcast.23, bf16[64,2048]{1,0:T(8,128)(2,1)} %bitcast.24, f32[1,64]{1,0:T(1,128)} %bitcast.30, ...), custom_call_target="tpu_custom_call" | custom-call | flops 134217728 | bytes 8388608 | tf_op jit(solution)/shard_map/attention/pallas_call | solution.py:480
  7.3 7.3 %all-to-all-start = ((bf16[32,8,768]{2,1,0:T(8,128)(2,1)}), bf16[32,8,768]{2,1,0:T(8,128)(2,1)S(1)}, u32[]{:S(2)}, u32[]{:S(2)}) async-start(bf16[32,8,768]{2,1,0:T(8,128)(2,1)} %bitcast.21), calls=%async_computation | async-start | bytes 786432 | tf_op jit(solution)/shard_map/all_to_all | solution.py:528
  14.7 5.8 %all-gather = bf16[128,256]{1,0:T(8,128)(2,1)} all-gather(bf16[32,256]{1,0:T(8,128)(2,1)S(1)} %get-tuple-element.14), channel_id=2, replica_groups=mesh['ep'=8,'tp'=4] {'tp'}, dimensions={0}, use_global_device_ids=true | all-gather | bytes 81920 | tf_op jit(solution)/shard_map/all_gather | solution.py:530
  20.5 4.4 %own.1 = (bf16[32,512]{1,0:T(8,128)(2,1)S(1)}, bf16[32,512]{1,0:T(8,128)(2,1)S(1)}, bf16[32,512]{1,0:T(8,128)(2,1)S(1)}, f32[32,512]{1,0:T(8,128)S(1)}, bf16[64,...) custom-call(bf16[4,32,256]{2,1,0:T(8,128)(2,1)} %bitcast.22, ...), custom_call_target="tpu_custom_call" | custom-call | flops 134217728 | bytes 12582912 | tf_op jit(solution)/shard_map/own/pallas_call | solution.py:540
  25.0 3.0 %all-to-all-done = bf16[32,8,768]{2,1,0:T(8,128)(2,1)S(1)} async-done(((bf16[32,8,768]{2,1,0:T(8,128)(2,1)}), bf16[32,8,768]{2,1,0:T(8,128)(2,1)S(1)}, u32[]{:S(2)}, u32[]{:S(2)}) %all-to-all-start) | async-done | bytes 393248 | tf_op jit(solution)/shard_map/all_to_all | solution.py:528
  27.9 5.3 %experts.1 = bf16[256,512]{1,0:T(8,128)(2,1)} custom-call(bf16[8,32,768]{2,1,0:T(8,128)(2,1)S(1)} %bitcast.15, f32[1,2048]{1,0:T(1,128)S(1)} %get-tuple-element.18.gain_ref, bf16[1024,512]{1,0:T(8,128)(2,1)S(1)} %get-tuple-element.19.refs_0_, bf16[1024,2048]{1,0:T(8,128)(2,1)} %refs_1_.1, bf16[2048,512]{1,0:T(8,128)(2,1)} %bitcast.17, ...), custom_call_target="tpu_custom_call" | custom-call | flops 671088640 | bytes 1048576 | tf_op jit(solution)/shard_map/experts/pallas_call | solution.py:590
  33.3 3.2 %all-to-all-start.1 = ((bf16[32,8,512]{2,1,0:T(8,128)(2,1)}), bf16[32,8,512]{2,1,0:T(8,128)(2,1)S(1)}, u32[]{:S(2)}, u32[]{:S(2)}) async-start(bf16[32,8,512]{2,1,0:T(8,128)(2,1)} %bitcast.20), calls=%async_computation.1 | async-start | bytes 524288 | tf_op jit(solution)/shard_map/all_to_all | solution.py:613
  36.5 0.3 collective-permute-start
  36.8 1.6 %collective-permute-start.1 = (bf16[32,512]{1,0:T(8,128)(2,1)S(1)}, bf16[32,512]{1,0:T(8,128)(2,1)S(1)}, u32[]{:S(2)}, u32[]{:S(2)}) collective-permute-start(bf16[32,512]{1,0:T(8,128)(2,1)S(1)} %get-tuple-element.21), channel_id=1, source_target_pairs={{0,2},{1,3},{2,0},{3,1},{4,6},{5,7},{6,4},{7,5},{8,10},{9,11},{10,... | collective-permute-start | bytes 98312 | tf_op jit(solution)/shard_map/ppermute | solution.py:615
  38.5 0.0 collective-permute-start.2
  38.5 0.0 collective-permute-done.refs_0_
  38.5 2.6 %collective-permute-done.1.refs_1_ = bf16[32,512]{1,0:T(8,128)(2,1)S(1)} collective-permute-done((bf16[32,512]{1,0:T(8,128)(2,1)S(1)}, bf16[32,512]{1,0:T(8,128)(2,1)S(1)}, u32[]{:S(2)}, u32[]{:S(2)}) %collective-permute-start.1) | collective-permute-done | bytes 32800 | tf_op jit(solution)/shard_map/ppermute | solution.py:615
  41.1 1.4 %collective-permute-done.2.refs_2_ = bf16[32,512]{1,0:T(8,128)(2,1)S(1)} collective-permute-done((bf16[32,512]{1,0:T(8,128)(2,1)S(1)}, bf16[32,512]{1,0:T(8,128)(2,1)S(1)}, u32[]{:S(2)}, u32[]{:S(2)}) %collective-permute-start.2) | collective-permute-done | bytes 32800 | tf_op jit(solution)/shard_map/ppermute | solution.py:615
  42.5 4.6 %all-to-all-done.1 = bf16[32,8,512]{2,1,0:T(8,128)(2,1)S(1)} async-done(((bf16[32,8,512]{2,1,0:T(8,128)(2,1)}), bf16[32,8,512]{2,1,0:T(8,128)(2,1)S(1)}, u32[]{:S(2)}, u32[]{:S(2)}) %all-to-all-start.1) | async-done | bytes 262176 | tf_op jit(solution)/shard_map/all_to_all | solution.py:613
  47.1 0.8 %combine.1 = bf16[32,512]{1,0:T(8,128)(2,1)} custom-call(f32[32,512]{1,0:T(8,128)S(1)} %get-tuple-element.15.base_ref, bf16[64,256]{1,0:T(8,128)(2,1)S(1)} %get-tuple-element.16.mix_ref, bf16[256,512]{1,0:T(8,128)(2,1)S(1)} %bitcast.16, bf16[32,512]{1,0:T(8,128)(2,1)S(1)} %collective-permute-done.refs_0_, ...), custom_call_target="tpu_custom_call" | custom-call | tf_op jit(solution)/shard_map/combine/pallas_call | solution.py:619
Async XLA Ops:
  7.3 20.6 %all-to-all-start = ((bf16[32,8,768]{2,1,0:T(8,128)(2,1)}), bf16[32,8,768]{2,1,0:T(8,128)(2,1)S(1)}, u32[]{:S(2)}, u32[]{:S(2)}) async-start(bf16[32,8,768]{2,1,0:T(8,128)(2,1)} %bitcast.21), calls=%async_computation | async-start | bytes 786432 | tf_op jit(solution)/shard_map/all_to_all | solution.py:528
  33.3 13.8 %all-to-all-start.1 = ((bf16[32,8,512]{2,1,0:T(8,128)(2,1)}), bf16[32,8,512]{2,1,0:T(8,128)(2,1)S(1)}, u32[]{:S(2)}, u32[]{:S(2)}) async-start(bf16[32,8,512]{2,1,0:T(8,128)(2,1)} %bitcast.20), calls=%async_computation.1 | async-start | bytes 524288 | tf_op jit(solution)/shard_map/all_to_all | solution.py:613
  36.5 2.0 %collective-permute-start = (bf16[32,512]{1,0:T(8,128)(2,1)S(1)}, bf16[32,512]{1,0:T(8,128)(2,1)S(1)}, u32[]{:S(2)}, u32[]{:S(2)}) collective-permute-start(bf16[32,512]{1,0:T(8,128)(2,1)S(1)} %get-tuple-element.20), channel_id=1, source_target_pairs={{0,1},{1,0},{2,3},{3,2},{4,5},{5,4},{6,7},{7,6},{8,9},{9,8},{10,11... | collective-permute-start | bytes 98312 | tf_op jit(solution)/shard_map/ppermute | solution.py:615
  36.8 4.3 %collective-permute-start.1 = (bf16[32,512]{1,0:T(8,128)(2,1)S(1)}, bf16[32,512]{1,0:T(8,128)(2,1)S(1)}, u32[]{:S(2)}, u32[]{:S(2)}) collective-permute-start(bf16[32,512]{1,0:T(8,128)(2,1)S(1)} %get-tuple-element.21), channel_id=1, source_target_pairs={{0,2},{1,3},{2,0},{3,1},{4,6},{5,7},{6,4},{7,5},{8,10},{9,11},{10,... | collective-permute-start | bytes 98312 | tf_op jit(solution)/shard_map/ppermute | solution.py:615
  38.5 4.1 %collective-permute-start.2 = (bf16[32,512]{1,0:T(8,128)(2,1)S(1)}, bf16[32,512]{1,0:T(8,128)(2,1)S(1)}, u32[]{:S(2)}, u32[]{:S(2)}) collective-permute-start(bf16[32,512]{1,0:T(8,128)(2,1)S(1)} %get-tuple-element.22), channel_id=1, source_target_pairs={{0,3},{1,2},{2,1},{3,0},{4,7},{5,6},{6,5},{7,4},{8,11},{9,10},{10,... | collective-permute-start | bytes 98312 | tf_op jit(solution)/shard_map/ppermute | solution.py:615

commit v4 on v3

--- a/solution.py
+++ b/solution.py
@@ -167,67 +167,80 @@
             keep = own_keys & (inner >= m * qk_width) & (inner < (m + 1) * qk_width)
             q_scr[:, m * heads + h, :] = jnp.where(keep, pair, 0.0)
 
-    row = iota((2 * rows, 1), 0) % rows
-    sign = jnp.where(row < heads, 1.0, 0.0)
+    row = iota((2 * rows, 1), 0)
+    sign = jnp.where(row < rows, 1.0, 0.0)
     for h in range(heads):
-        sign = jnp.where(row == heads + h, -lambdas_ref[h], sign)
+        sign = jnp.where((row >= rows) & (row % heads == h), -lambdas_ref[h], sign)
     position = iota((2 * rows, cache_len), 1)
-    second = iota((2 * rows, 1), 0) >= rows
+    second = row % rows >= heads
+
+    def query_of(s):
+        even, odd = q_scr[s], q_scr[s + 1]
+        return jnp.concatenate([even[:heads], odd[:heads], even[heads:], odd[heads:]], axis=0)
 
     def scores_of(step):
         found = []
         for b in range(0, block, 2):
             s = step * block + b
             even, odd = kv_ref[s], kv_ref[s + 1]
-            query = q_scr[s : s + 2].reshape(2 * rows, lanes).astype(bf16)
+            query = query_of(s)
             keys = jnp.concatenate([even[:, :v_width], odd[:, :v_width]], axis=1)
             values = jnp.concatenate([odd[:, v_width:], even[:, v_width:]], axis=1)
-            found.append((dot_nt(query, keys), values))
+            fresh = query * jnp.where(second, k_scr[s + 1 : s + 2], k_scr[s : s + 1])
+            fresh = jnp.sum(fresh, axis=1, keepdims=True)
+            found.append((dot_nt(query.astype(bf16), keys), fresh, values))
         return found
 
-    def fold(part):
-        halves = [part[i * rows : (i + 1) * rows] for i in range(2)]
-        return jnp.concatenate([half + pltpu.roll(half, heads, 0) for half in halves], axis=0)
-
-    def finish(step, found):
+    def weights_of(step, found):
+        made = []
         for b in range(0, block, 2):
             s = step * block + b
+            scores, fresh, values = found[b // 2]
             length = jnp.where(second, lengths_ref[s + 1], lengths_ref[s])
-            scores = jnp.where(position < length, found[b // 2][0] * scaling, neg_fill)
-            fresh = jnp.sum(q_scr[s : s + 2] * k_scr[s : s + 2][:, None, :], axis=2, keepdims=True)
-            fresh = fresh.reshape(2 * rows, 1) * scaling
+            scores = jnp.where(position < length, scores * scaling, neg_fill)
+            fresh = fresh * scaling
             top = jnp.maximum(jnp.max(scores, axis=1, keepdims=True), fresh)
             expo = jnp.exp(scores - top)
             expo_new = jnp.exp(fresh - top)
             factor = sign / (jnp.sum(expo, axis=1, keepdims=True) + expo_new)
-            part_new = jnp.broadcast_to(expo_new * factor, (2 * rows, lanes))
-            weights = fold(expo * factor).astype(bf16)
-            weight_new = fold(part_new).astype(bf16).astype(f32)
-            mixed = dot(weights, found[b // 2][1]).reshape(2, rows, lanes)
-            o_scr[s : s + 2] = (
-                mixed + weight_new.reshape(2, rows, lanes) * v_scr[s : s + 2][:, None, :]
-            )
-
-    held = None
-    for step in range(steps + 1):
+            part = expo * factor
+            part_new = expo_new * factor
+            weights = (part[:rows] + part[rows:]).astype(bf16)
+            weight_new = (part_new[:rows] + part_new[rows:]).astype(bf16).astype(f32)
+            value_new = jnp.where(second[:rows], v_scr[s + 1 : s + 2], v_scr[s : s + 1])
+            made.append((weights, weight_new * value_new, values))
+        return made
+
+    def mix_values(step, made):
+        for b in range(0, block, 2):
+            weights, newest, values = made[b // 2]
+            o_scr[(step * block + b) // 2] = dot(weights, values) + newest
+
+    found, made = None, None
+    for step in range(steps + 2):
         if step < steps:
             streams[step].wait()
+        if step >= 2:
+            mix_values(step - 2, made)
+        if 1 <= step <= steps:
+            made = weights_of(step - 1, found)
+        if step < steps:
             found = scores_of(step)
-        if step:
-            finish(step - 1, held)
-        held = found
-
-    outs = []
-    for h in range(heads):
-        mix = jnp.where(own_keys, 0.0, o_scr[:, h, :])
-        mean = jnp.sum(mix * mix, axis=1, keepdims=True) * (1.0 / v_width)
-        mix = mix * lax.rsqrt(mean + epsilon)
-        outs.append(mix + pltpu.roll(mix, v_width, 1))
+
     gains = jnp.concatenate([head_gain_ref[...], head_gain_ref[...]], axis=1)
-    pairs = [
-        jnp.where(upper, outs[2 * p + 1], outs[2 * p]) * gains for p in range(heads // 2)
-    ]
-    head_out = jnp.concatenate(pairs, axis=1).astype(bf16)
+    half = upper[: seqs // 2]
+    for i in range(2):
+        outs = []
+        for h in range(heads):
+            mix = jnp.where(half == (i == 0), o_scr[:, i * heads + h, :], 0.0)
+            mean = jnp.sum(mix * mix, axis=1, keepdims=True) * (1.0 / v_width)
+            mix = mix * lax.rsqrt(mean + epsilon)
+            turned = pltpu.roll(mix, v_width, 1)
+            outs.append((turned, mix) if i == 0 else (mix, turned))
+        for p in range(heads // 2):
+            out = jnp.where(half, outs[2 * p + 1][1], outs[2 * p][0]) * gains
+            q_scr[i :: 2, p, :] = out
+    head_out = jnp.concatenate([q_scr[:, p, :] for p in range(heads // 2)], axis=1).astype(bf16)
     heads_ref[...] = head_out
     mix_scr[...] = dot(picks, head_out).astype(bf16)
     backs[1].start()
@@ -499,7 +512,7 @@
             pltpu.VMEM((seqs, 2 * heads, lanes), f32),
             pltpu.VMEM((seqs, lanes), f32),
             pltpu.VMEM((seqs, lanes), f32),
-            pltpu.VMEM((seqs, 2 * heads, lanes), f32),
+            pltpu.VMEM((seqs // 2, 2 * heads, lanes), f32),
             pltpu.VMEM((routing.shape[0], 8), f32),
             pltpu.VMEM((devices * capacity, share), bf16),
             pltpu.VMEM((devices * capacity, local), bf16),

time: 48.2 us -> 47.4 us (0.983)
  Pallas kernels: 17.9 us -> 17.1 us
    pallas_call x1, Pallas kernels: 7.34 us -> 6.56 us  [shards(): pl.pallas_call(functools.partial(attention_kernel, capacity, experts, blo...]
where the time goes in v4:
time: 47.4 us; the launch traced here: 47.1 us
  Pallas kernels  17.1 us (36%)
  starting transfers between devices  12.5 us (26%)
  waiting for transfers between devices  11.6 us (24%)
  blocking collectives  5.82 us (12%)
    all_to_all x1, starting transfers between devices, shards(): lax.all_to_all(send, ('ep', 'tp'), split_axis=0, concat_axis=0, tiled=True)  7.33 us
    pallas_call x1, Pallas kernels, shards(): pl.pallas_call(functools.partial(attention_kernel, capacity, experts, blo...  6.56 us
    all_gather x1, blocking collectives, shards(): all_heads = lax.all_gather(head_out, 'tp', axis=0, tiled=False)  5.82 us
    pallas_call x1, Pallas kernels, shards(): pl.pallas_call(functools.partial(expert_kernel, direct, kept), in_specs=[...  5.32 us
    all_to_all x1, waiting for transfers between devices, shards(): lax.all_to_all(sent, ('ep', 'tp'), split_axis=0, concat_axis=0, tiled=True)  4.57 us
    pallas_call x1, Pallas kernels, shards(): pl.pallas_call(functools.partial(own_kernel, capacity, experts, kept), in...  4.42 us
    ppermute x3, waiting for transfers between devices, shards(): lax.ppermute(piece, 'tp', [(i, partner(i, d, tp_count)) for i in range(tp...  4.05 us
    all_to_all x1, starting transfers between devices, shards(): lax.all_to_all(sent, ('ep', 'tp'), split_axis=0, concat_axis=0, tiled=True)  3.25 us
  transfers between devices with their start and end apart: 5, of which 4 were waited for; matrix products, arithmetic and copies ran while one was open for 0% of the time, Pallas kernels for 9%

profile of v4, /device:TPU:0, one launch (start us, length us, event | category | flops | bytes accessed | tf_op | source)
XLA Modules:
  0.0 47.1 jit_solution(16011582158921840007)
XLA Ops:
  0.0 6.6 %attention.1 = (bf16[32,256]{1,0:T(8,128)(2,1)S(1)}, bf16[256,768]{1,0:T(8,128)(2,1)}) custom-call(bf16[32,2048]{1,0:T(8,128)(2,1)} %tokens_hbm.3, f32[1,2048]{1,0:T(1,128)} %bitcast.28, bf16[2048,256]{1,0:T(8,128)(2,1)} %w_query_hbm.1, bf16[64,2048]{1,0:T(8,128)(2,1)} %bitcast.23, bf16[64,2048]{1,0:T(8,128)(2,1)} %bitcast.24, f32[1,64]{1,0:T(1,128)} %bitcast.30, ...), custom_call_target="tpu_custom_call" | custom-call | flops 134217728 | bytes 8388608 | tf_op jit(solution)/shard_map/attention/pallas_call | solution.py:493
  6.6 7.3 %all-to-all-start = ((bf16[32,8,768]{2,1,0:T(8,128)(2,1)}), bf16[32,8,768]{2,1,0:T(8,128)(2,1)S(1)}, u32[]{:S(2)}, u32[]{:S(2)}) async-start(bf16[32,8,768]{2,1,0:T(8,128)(2,1)} %bitcast.21), calls=%async_computation | async-start | bytes 786432 | tf_op jit(solution)/shard_map/all_to_all | solution.py:541
  13.9 5.8 %all-gather = bf16[128,256]{1,0:T(8,128)(2,1)} all-gather(bf16[32,256]{1,0:T(8,128)(2,1)S(1)} %get-tuple-element.14), channel_id=2, replica_groups=mesh['ep'=8,'tp'=4] {'tp'}, dimensions={0}, use_global_device_ids=true | all-gather | bytes 81920 | tf_op jit(solution)/shard_map/all_gather | solution.py:543
  19.7 4.4 %own.1 = (bf16[32,512]{1,0:T(8,128)(2,1)S(1)}, bf16[32,512]{1,0:T(8,128)(2,1)S(1)}, bf16[32,512]{1,0:T(8,128)(2,1)S(1)}, f32[32,512]{1,0:T(8,128)S(1)}, bf16[64,...) custom-call(bf16[4,32,256]{2,1,0:T(8,128)(2,1)} %bitcast.22, ...), custom_call_target="tpu_custom_call" | custom-call | flops 134217728 | bytes 12582912 | tf_op jit(solution)/shard_map/own/pallas_call | solution.py:553
  24.2 3.0 %all-to-all-done = bf16[32,8,768]{2,1,0:T(8,128)(2,1)S(1)} async-done(((bf16[32,8,768]{2,1,0:T(8,128)(2,1)}), bf16[32,8,768]{2,1,0:T(8,128)(2,1)S(1)}, u32[]{:S(2)}, u32[]{:S(2)}) %all-to-all-start) | async-done | bytes 393248 | tf_op jit(solution)/shard_map/all_to_all | solution.py:541
  27.2 5.3 %experts.1 = bf16[256,512]{1,0:T(8,128)(2,1)} custom-call(bf16[8,32,768]{2,1,0:T(8,128)(2,1)S(1)} %bitcast.15, f32[1,2048]{1,0:T(1,128)S(1)} %get-tuple-element.18.gain_ref, bf16[1024,512]{1,0:T(8,128)(2,1)S(1)} %get-tuple-element.19.refs_0_, bf16[1024,2048]{1,0:T(8,128)(2,1)} %refs_1_.1, bf16[2048,512]{1,0:T(8,128)(2,1)} %bitcast.17, ...), custom_call_target="tpu_custom_call" | custom-call | flops 671088640 | bytes 1048576 | tf_op jit(solution)/shard_map/experts/pallas_call | solution.py:603
  32.5 3.2 %all-to-all-start.1 = ((bf16[32,8,512]{2,1,0:T(8,128)(2,1)}), bf16[32,8,512]{2,1,0:T(8,128)(2,1)S(1)}, u32[]{:S(2)}, u32[]{:S(2)}) async-start(bf16[32,8,512]{2,1,0:T(8,128)(2,1)} %bitcast.20), calls=%async_computation.1 | async-start | bytes 524288 | tf_op jit(solution)/shard_map/all_to_all | solution.py:626
  35.7 0.3 collective-permute-start
  36.1 1.6 %collective-permute-start.1 = (bf16[32,512]{1,0:T(8,128)(2,1)S(1)}, bf16[32,512]{1,0:T(8,128)(2,1)S(1)}, u32[]{:S(2)}, u32[]{:S(2)}) collective-permute-start(bf16[32,512]{1,0:T(8,128)(2,1)S(1)} %get-tuple-element.21), channel_id=1, source_target_pairs={{0,2},{1,3},{2,0},{3,1},{4,6},{5,7},{6,4},{7,5},{8,10},{9,11},{10,... | collective-permute-start | bytes 98312 | tf_op jit(solution)/shard_map/ppermute | solution.py:628
  37.7 0.0 collective-permute-start.2
  37.7 0.0 collective-permute-done.refs_0_
  37.7 2.6 %collective-permute-done.1.refs_1_ = bf16[32,512]{1,0:T(8,128)(2,1)S(1)} collective-permute-done((bf16[32,512]{1,0:T(8,128)(2,1)S(1)}, bf16[32,512]{1,0:T(8,128)(2,1)S(1)}, u32[]{:S(2)}, u32[]{:S(2)}) %collective-permute-start.1) | collective-permute-done | bytes 32800 | tf_op jit(solution)/shard_map/ppermute | solution.py:628
  40.3 1.4 %collective-permute-done.2.refs_2_ = bf16[32,512]{1,0:T(8,128)(2,1)S(1)} collective-permute-done((bf16[32,512]{1,0:T(8,128)(2,1)S(1)}, bf16[32,512]{1,0:T(8,128)(2,1)S(1)}, u32[]{:S(2)}, u32[]{:S(2)}) %collective-permute-start.2) | collective-permute-done | bytes 32800 | tf_op jit(solution)/shard_map/ppermute | solution.py:628
  41.7 4.6 %all-to-all-done.1 = bf16[32,8,512]{2,1,0:T(8,128)(2,1)S(1)} async-done(((bf16[32,8,512]{2,1,0:T(8,128)(2,1)}), bf16[32,8,512]{2,1,0:T(8,128)(2,1)S(1)}, u32[]{:S(2)}, u32[]{:S(2)}) %all-to-all-start.1) | async-done | bytes 262176 | tf_op jit(solution)/shard_map/all_to_all | solution.py:626
  46.3 0.8 %combine.1 = bf16[32,512]{1,0:T(8,128)(2,1)} custom-call(f32[32,512]{1,0:T(8,128)S(1)} %get-tuple-element.15.base_ref, bf16[64,256]{1,0:T(8,128)(2,1)S(1)} %get-tuple-element.16.mix_ref, bf16[256,512]{1,0:T(8,128)(2,1)S(1)} %bitcast.16, bf16[32,512]{1,0:T(8,128)(2,1)S(1)} %collective-permute-done.refs_0_, ...), custom_call_target="tpu_custom_call" | custom-call | tf_op jit(solution)/shard_map/combine/pallas_call | solution.py:632
Async XLA Ops:
  6.6 20.6 %all-to-all-start = ((bf16[32,8,768]{2,1,0:T(8,128)(2,1)}), bf16[32,8,768]{2,1,0:T(8,128)(2,1)S(1)}, u32[]{:S(2)}, u32[]{:S(2)}) async-start(bf16[32,8,768]{2,1,0:T(8,128)(2,1)} %bitcast.21), calls=%async_computation | async-start | bytes 786432 | tf_op jit(solution)/shard_map/all_to_all | solution.py:541
  32.5 13.8 %all-to-all-start.1 = ((bf16[32,8,512]{2,1,0:T(8,128)(2,1)}), bf16[32,8,512]{2,1,0:T(8,128)(2,1)S(1)}, u32[]{:S(2)}, u32[]{:S(2)}) async-start(bf16[32,8,512]{2,1,0:T(8,128)(2,1)} %bitcast.20), calls=%async_computation.1 | async-start | bytes 524288 | tf_op jit(solution)/shard_map/all_to_all | solution.py:626
  35.7 2.0 %collective-permute-start = (bf16[32,512]{1,0:T(8,128)(2,1)S(1)}, bf16[32,512]{1,0:T(8,128)(2,1)S(1)}, u32[]{:S(2)}, u32[]{:S(2)}) collective-permute-start(bf16[32,512]{1,0:T(8,128)(2,1)S(1)} %get-tuple-element.20), channel_id=1, source_target_pairs={{0,1},{1,0},{2,3},{3,2},{4,5},{5,4},{6,7},{7,6},{8,9},{9,8},{10,11... | collective-permute-start | bytes 98312 | tf_op jit(solution)/shard_map/ppermute | solution.py:628
  36.1 4.3 %collective-permute-start.1 = (bf16[32,512]{1,0:T(8,128)(2,1)S(1)}, bf16[32,512]{1,0:T(8,128)(2,1)S(1)}, u32[]{:S(2)}, u32[]{:S(2)}) collective-permute-start(bf16[32,512]{1,0:T(8,128)(2,1)S(1)} %get-tuple-element.21), channel_id=1, source_target_pairs={{0,2},{1,3},{2,0},{3,1},{4,6},{5,7},{6,4},{7,5},{8,10},{9,11},{10,... | collective-permute-start | bytes 98312 | tf_op jit(solution)/shard_map/ppermute | solution.py:628
  37.7 4.1 %collective-permute-start.2 = (bf16[32,512]{1,0:T(8,128)(2,1)S(1)}, bf16[32,512]{1,0:T(8,128)(2,1)S(1)}, u32[]{:S(2)}, u32[]{:S(2)}) collective-permute-start(bf16[32,512]{1,0:T(8,128)(2,1)S(1)} %get-tuple-element.22), channel_id=1, source_target_pairs={{0,3},{1,2},{2,1},{3,0},{4,7},{5,6},{6,5},{7,4},{8,11},{9,10},{10,... | collective-permute-start | bytes 98312 | tf_op jit(solution)/shard_map/ppermute | solution.py:628

commit v5 on v4

--- a/solution.py
+++ b/solution.py
@@ -257,55 +257,92 @@
 
 
 def own_kernel(
-    capacity,
-    experts,
-    kept,
     heads_ref,
     w_out_hbm,
     tokens_hbm,
     gain_hbm,
-    s_gate_hbm,
-    s_up_hbm,
-    s_down_hbm,
+    ffn_ref,
+    base_ref,
+    gain_ref,
+    kept_ref,
+    tokens_ref,
+    rest_ref,
+    res_scr,
+    sems,
+):
+    tp_count, seqs, width = heads_ref.shape
+    share = base_ref.shape[1]
+    blocks = column_blocks(w_out_hbm, rest_ref, (kept_ref,))
+    copies = [
+        pltpu.make_async_copy(source, target, sems.at[i])
+        for i, (source, target) in enumerate(
+            [(tokens_hbm, tokens_ref), (gain_hbm, gain_ref), *blocks]
+        )
+    ]
+    for copy in copies:
+        copy.start()
+    for copy in copies[:2]:
+        copy.wait()
+    square = jnp.zeros((seqs, 1), f32)
+    for n, (_, w_out_ref) in enumerate(blocks):
+        copies[2 + n].wait()
+        cut = slice(n * share, (n + 1) * share)
+        total = tokens_ref[:, cut].astype(f32)
+        parts = jnp.zeros_like(total)
+        for j in range(tp_count):
+            part = dot(heads_ref[j], w_out_ref[j * width : (j + 1) * width])
+            parts = parts + part.astype(bf16).astype(f32)
+        residual = (total + parts).astype(bf16).astype(f32)
+        res_scr[:, cut] = residual
+        square = square + jnp.sum(residual * residual, axis=1, keepdims=True)
+    scale = lax.rsqrt(square * (1.0 / res_scr.shape[1]) + epsilon)
+    start = pl.multiple_of(lax.axis_index("tp") * share, share)
+    base_ref[...] = res_scr[:, pl.ds(start, share)]
+    ffn_ref[...] = (res_scr[...] * scale * gain_ref[...]).astype(bf16)
+
+
+def shared_kernel(
+    capacity,
+    experts,
+    ffn_ref,
+    residual_ref,
+    _,
+    gate_hbm,
+    up_hbm,
+    down_hbm,
     routing_hbm,
     rates_hbm,
     *refs,
 ):
-    tp_count, seqs, width = heads_ref.shape
+    seqs, share = residual_ref.shape
+    tp_count = ffn_ref.shape[1] // share
     part_refs = refs[: tp_count - 1]
-    base_ref, mix_ref, gain_ref, *kept_refs = refs[tp_count - 1 : tp_count + 2 + kept]
-    refs = refs[tp_count + 2 + kept :]
     (
-        tokens_ref,
-        rest_ref,
-        s_gate_ref,
-        s_up_ref,
-        s_down_ref,
+        base_ref,
+        mix_ref,
+        gate_ref,
+        up_ref,
+        down_ref,
         routing_ref,
         rates_ref,
-        res_scr,
         slot_scr,
         sems,
-    ) = refs
-    share = base_ref.shape[1]
-    blocks = column_blocks(w_out_hbm, rest_ref, kept_refs)
-    early = [
-        (tokens_hbm, tokens_ref),
-        (gain_hbm, gain_ref),
-        (routing_hbm, routing_ref),
-        (rates_hbm, rates_ref),
-        *blocks,
-        (s_gate_hbm, s_gate_ref),
-        (s_up_hbm, s_up_ref),
-        (s_down_hbm, s_down_ref),
-    ]
+    ) = refs[tp_count - 1 :]
     copies = [
         pltpu.make_async_copy(source, target, sems.at[i])
-        for i, (source, target) in enumerate(early)
+        for i, (source, target) in enumerate(
+            [
+                (routing_hbm, routing_ref),
+                (rates_hbm, rates_ref),
+                (gate_hbm, gate_ref),
+                (up_hbm, up_ref),
+                (down_hbm, down_ref),
+            ]
+        )
     ]
     for copy in copies:
         copy.start()
-    for copy in copies[:4]:
+    for copy in copies[:2]:
         copy.wait()
     slots = own_slots(routing_ref, slot_scr, seqs, experts, capacity)
     top_count = rates_ref.shape[0]
@@ -318,33 +355,19 @@
     high = mixing.astype(bf16)
     mix_ref[:seqs] = high
     mix_ref[seqs:] = (mixing - high.astype(f32)).astype(bf16)
-
-    square = jnp.zeros((seqs, 1), f32)
-    for n in range(tp_count):
-        copies[4 + n].wait()
-        w_out_ref = blocks[n][1]
-        cut = slice(n * share, (n + 1) * share)
-        total = tokens_ref[:, cut].astype(f32)
-        parts = jnp.zeros((seqs, share), f32)
-        for j in range(tp_count):
-            part = dot(heads_ref[j], w_out_ref[j * width : (j + 1) * width])
-            parts = parts + part.astype(bf16).astype(f32)
-        residual = (total + parts).astype(bf16).astype(f32)
-        res_scr[:, cut] = residual
-        square = square + jnp.sum(residual * residual, axis=1, keepdims=True)
-    scale = lax.rsqrt(square * (1.0 / res_scr.shape[1]) + epsilon)
-    ffn_in = (res_scr[...] * scale * gain_ref[...]).astype(bf16)
-    for copy in copies[4 + tp_count :]:
+    for copy in copies[2:4]:
         copy.wait()
-    act = silu(dot(ffn_in, s_gate_ref[...])) * dot(ffn_in, s_up_ref[...])
+    ffn_in = ffn_ref[...]
+    act = silu(dot(ffn_in, gate_ref[...])) * dot(ffn_in, up_ref[...])
     act = act.astype(bf16)
+    copies[4].wait()
     for d in range(tp_count):
         start = pl.multiple_of(partner(lax.axis_index("tp"), d, tp_count) * share, share)
-        part = dot(act, s_down_ref[:, pl.ds(start, share)])
+        part = dot(act, down_ref[:, pl.ds(start, share)])
         if d:
             part_refs[d - 1][...] = part.astype(bf16)
         else:
-            base_ref[...] = res_scr[:, pl.ds(start, share)] + part
+            base_ref[...] = residual_ref[...] + part
 
 
 def column_blocks(w_out_hbm, rest_ref, kept_refs):
@@ -546,63 +569,38 @@
     exp_up = w_exp_up.reshape(w_exp_up.shape[1:])
     exp_down = w_exp_down.reshape(w_exp_down.shape[1:])
     rows = ep_count * capacity
-    slot_count = experts * capacity
-    kept = 1
     w_out_block = (w_out.shape[0], share)
-    rest = pltpu.VMEM((tp_count - kept, *w_out_block), bf16)
-    results = pl.pallas_call(
-        functools.partial(own_kernel, capacity, experts, kept),
-        in_specs=[VMEM] + [HBM] * 8,
-        out_specs=[VMEM] * (tp_count + 2 + kept),
-        out_shape=[pltpu.VMEM((seqs, share), bf16)] * (tp_count - 1)
-        + [
+    rest = pltpu.VMEM((tp_count - 1, *w_out_block), bf16)
+    ffn_own, residual, gain, kept = pl.pallas_call(
+        own_kernel,
+        in_specs=[VMEM] + [HBM] * 3,
+        out_specs=[VMEM] * 4,
+        out_shape=[
+            pltpu.VMEM((seqs, width), bf16),
             pltpu.VMEM((seqs, share), f32),
-            pltpu.VMEM((2 * seqs, slot_count), bf16),
             pltpu.VMEM((1, width), f32),
-        ]
-        + [pltpu.VMEM(w_out_block, bf16)] * kept,
+            pltpu.VMEM(w_out_block, bf16),
+        ],
         scratch_shapes=[
             pltpu.VMEM(tokens.shape, bf16),
             rest,
-            pltpu.VMEM(w_shared_gate.shape, bf16),
-            pltpu.VMEM(w_shared_up.shape, bf16),
-            pltpu.VMEM(w_shared_down.shape, bf16),
-            pltpu.VMEM(routing.shape[::-1], jnp.int32),
-            pltpu.VMEM(route_weights.shape[::-1], f32),
             pltpu.VMEM((seqs, width), f32),
-            pltpu.VMEM((routing.shape[0], 8), f32),
-            pltpu.SemaphoreType.DMA((7 + tp_count,)),
+            pltpu.SemaphoreType.DMA((2 + tp_count,)),
         ],
         compiler_params=pltpu.CompilerParams(vmem_limit_bytes=63_900_000),
         cost_estimate=pl.CostEstimate(
-            flops=2 * seqs * w_out.size, bytes_accessed=12 << 20, transcendentals=0
+            flops=2 * seqs * w_out.size, bytes_accessed=4 << 20, transcendentals=0
         ),
         name="own",
-    )(
-        all_heads,
-        w_out,
-        tokens,
-        ffn_gain.reshape(1, width),
-        w_shared_gate,
-        w_shared_up,
-        w_shared_down,
-        routing.T,
-        route_weights.T,
-    )
-
-    part, (base, mix, gain), kept_blocks = (
-        results[: tp_count - 1],
-        results[tp_count - 1 : tp_count + 2],
-        results[tp_count + 2 :],
-    )
-    arrived, gain, *kept_blocks = [
-        pltpu.with_memory_space_constraint(value, pltpu.VMEM)
-        for value in (arrived, gain, *kept_blocks)
-    ]
+    )(all_heads, w_out, tokens, ffn_gain.reshape(1, width))
+    arrived, gain, kept = [
+        pltpu.with_memory_space_constraint(value, pltpu.VMEM) for value in (arrived, gain, kept)
+    ]
+
     sent_shape = (devices * capacity, share) if direct else (rows, width)
     sent = pl.pallas_call(
-        functools.partial(expert_kernel, direct, kept),
-        in_specs=[VMEM] * (2 + kept) + [HBM] * 4,
+        functools.partial(expert_kernel, direct, 1),
+        in_specs=[VMEM] * 3 + [HBM] * 4,
         out_specs=HBM,
         out_shape=jax.ShapeDtypeStruct(sent_shape, bf16),
         scratch_shapes=[
@@ -612,18 +610,51 @@
             pltpu.VMEM(exp_up.shape, bf16),
             pltpu.VMEM((tp_count, exp_down.shape[0], share), bf16),
             pltpu.VMEM((rows, width), f32),
-            pltpu.SemaphoreType.DMA((2 + 2 * tp_count - kept,)),
+            pltpu.SemaphoreType.DMA((1 + 2 * tp_count,)),
         ],
         compiler_params=pltpu.CompilerParams(vmem_limit_bytes=60 * 1024 * 1024),
         cost_estimate=pl.CostEstimate(
             flops=2 * rows * 5 * w_out.size // 2, bytes_accessed=1 << 20, transcendentals=0
         ),
         name="experts",
-    )(arrived, gain, *kept_blocks, w_out, exp_gate, exp_up, exp_down)
+    )(arrived, gain, kept, w_out, exp_gate, exp_up, exp_down)
     if not direct:
         sent = sent.reshape(ep_count, capacity, tp_count, share)
         sent = sent.transpose(0, 2, 1, 3).reshape(devices * capacity, share)
     returned = lax.all_to_all(sent, ("ep", "tp"), split_axis=0, concat_axis=0, tiled=True)
+    *part, base, mix = pl.pallas_call(
+        functools.partial(shared_kernel, capacity, experts),
+        in_specs=[VMEM] * 2 + [HBM] * 6,
+        out_specs=[VMEM] * (tp_count + 1),
+        out_shape=[pltpu.VMEM((seqs, share), bf16)] * (tp_count - 1)
+        + [
+            pltpu.VMEM((seqs, share), f32),
+            pltpu.VMEM((2 * seqs, experts * capacity), bf16),
+        ],
+        scratch_shapes=[
+            pltpu.VMEM(w_shared_gate.shape, bf16),
+            pltpu.VMEM(w_shared_up.shape, bf16),
+            pltpu.VMEM(w_shared_down.shape, bf16),
+            pltpu.VMEM(routing.shape[::-1], jnp.int32),
+            pltpu.VMEM(route_weights.shape[::-1], f32),
+            pltpu.VMEM((routing.shape[0], 8), f32),
+            pltpu.SemaphoreType.DMA((5,)),
+        ],
+        compiler_params=pltpu.CompilerParams(vmem_limit_bytes=65_500_000),
+        cost_estimate=pl.CostEstimate(
+            flops=2 * seqs * 3 * w_shared_up.size, bytes_accessed=3 << 19, transcendentals=0
+        ),
+        name="shared",
+    )(
+        ffn_own,
+        residual,
+        sent,
+        w_shared_gate,
+        w_shared_up,
+        w_shared_down,
+        routing.T,
+        route_weights.T,
+    )
     parts = [
         lax.ppermute(piece, "tp", [(i, partner(i, d, tp_count)) for i in range(tp_count)])
         for d, piece in enumerate(part, 1)

time: 47.4 us -> 46.8 us (0.987)
  waiting for transfers between devices: 11.6 us -> 9.55 us
  Pallas kernels: 17.1 us -> 19.1 us
  starting transfers between devices: 12.5 us -> 11.9 us
    all_to_all x1, waiting for transfers between devices: 4.57 us -> 2.19 us  [shards(): lax.all_to_all(sent, ('ep', 'tp'), split_axis=0, concat_axis=0, tiled=True)]
    pallas_call x2 -> x3, Pallas kernels: 9.74 us -> 11.8 us  [the longest x1 5.33 us: shards(): pl.pallas_call(functools.partial(expert_kernel, direct, 1), in_specs=[VME...]
    all_to_all x1, waiting for transfers between devices: 2.99 us -> 3.64 us  [shards(): lax.all_to_all(send, ('ep', 'tp'), split_axis=0, concat_axis=0, tiled=True)]
    all_to_all x1, starting transfers between devices: 3.25 us -> 2.62 us  [shards(): lax.all_to_all(sent, ('ep', 'tp'), split_axis=0, concat_axis=0, tiled=True)]
  transfers between devices with their start and end apart: 5 -> 5, of which waited for: 4 -> 4; matrix products, arithmetic and copies ran while one was open for 0% -> 0% of each run, Pallas kernels for 9% -> 14%
where the time goes in v5:
time: 46.8 us; the launch traced here: 46.5 us
  Pallas kernels  19.1 us (41%)
  starting transfers between devices  11.9 us (25%)
  waiting for transfers between devices  9.55 us (20%)
  blocking collectives  5.82 us (12%)
    all_to_all x1, starting transfers between devices, shards(): lax.all_to_all(send, ('ep', 'tp'), split_axis=0, concat_axis=0, tiled=True)  7.33 us
    pallas_call x1, Pallas kernels, shards(): pl.pallas_call(functools.partial(attention_kernel, capacity, experts, blo...  6.56 us
    all_gather x1, blocking collectives, shards(): all_heads = lax.all_gather(head_out, 'tp', axis=0, tiled=False)  5.82 us
    pallas_call x1, Pallas kernels, shards(): pl.pallas_call(functools.partial(expert_kernel, direct, 1), in_specs=[VME...  5.33 us
    pallas_call x1, Pallas kernels, shards(): pl.pallas_call(own_kernel, in_specs=[VMEM] + [HBM] * 3, out_specs=[VMEM]...  3.75 us
    ppermute x3, waiting for transfers between devices, shards(): lax.ppermute(piece, 'tp', [(i, partner(i, d, tp_count)) for i in range(tp...  3.73 us
    all_to_all x1, waiting for transfers between devices, shards(): lax.all_to_all(send, ('ep', 'tp'), split_axis=0, concat_axis=0, tiled=True)  3.64 us
    pallas_call x1, Pallas kernels, shards(): pl.pallas_call(functools.partial(shared_kernel, capacity, experts), in_sp...  2.71 us
  transfers between devices with their start and end apart: 5, of which 4 were waited for; matrix products, arithmetic and copies ran while one was open for 0% of the time, Pallas kernels for 14%

profile of v5, /device:TPU:0, one launch (start us, length us, event | category | flops | bytes accessed | tf_op | source)
XLA Modules:
  0.0 46.5 jit_solution(4126189178885209765)
XLA Ops:
  0.0 6.6 %attention.1 = (bf16[32,256]{1,0:T(8,128)(2,1)S(1)}, bf16[256,768]{1,0:T(8,128)(2,1)}) custom-call(bf16[32,2048]{1,0:T(8,128)(2,1)} %tokens_hbm.3, f32[1,2048]{1,0:T(1,128)} %bitcast.28, bf16[2048,256]{1,0:T(8,128)(2,1)} %w_query_hbm.1, bf16[64,2048]{1,0:T(8,128)(2,1)} %bitcast.23, bf16[64,2048]{1,0:T(8,128)(2,1)} %bitcast.24, f32[1,64]{1,0:T(1,128)} %bitcast.30, ...), custom_call_target="tpu_custom_call" | custom-call | flops 134217728 | bytes 8388608 | tf_op jit(solution)/shard_map/attention/pallas_call | solution.py:516
  6.6 7.3 %all-to-all-start = ((bf16[32,8,768]{2,1,0:T(8,128)(2,1)}), bf16[32,8,768]{2,1,0:T(8,128)(2,1)S(1)}, u32[]{:S(2)}, u32[]{:S(2)}) async-start(bf16[32,8,768]{2,1,0:T(8,128)(2,1)} %bitcast.21), calls=%async_computation | async-start | bytes 786432 | tf_op jit(solution)/shard_map/all_to_all | solution.py:564
  13.9 5.8 %all-gather = bf16[128,256]{1,0:T(8,128)(2,1)} all-gather(bf16[32,256]{1,0:T(8,128)(2,1)S(1)} %get-tuple-element.16), channel_id=2, replica_groups=mesh['ep'=8,'tp'=4] {'tp'}, dimensions={0}, use_global_device_ids=true | all-gather | bytes 81920 | tf_op jit(solution)/shard_map/all_gather | solution.py:566
  19.7 3.8 %own.1 = (bf16[32,2048]{1,0:T(8,128)(2,1)S(1)}, f32[32,512]{1,0:T(8,128)S(1)}, f32[1,2048]{1,0:T(1,128)S(1)}, bf16[1024,512]{1,0:T(8,128)(2,1)S(1)}) custom-call(bf16[4,32,256]{2,1,0:T(8,128)(2,1)} %bitcast.22, bf16[1024,2048]{1,0:T(8,128)(2,1)} %refs_1_.1, bf16[32,2048]{1,0:T(8,128)(2,1)} %tokens_hbm.3, f32[1,2048]{1,0:T(1,128)} %bitcast.27), custom_call_target="tpu_custom_call" | custom-call | flops 134217728 | bytes 4194304 | tf_op jit(solution)/shard_map/own/pallas_call | solution.py:574
  23.5 0.0 copy-start
  23.5 0.0 copy-start.1
  23.5 3.6 %all-to-all-done = bf16[32,8,768]{2,1,0:T(8,128)(2,1)S(1)} async-done(((bf16[32,8,768]{2,1,0:T(8,128)(2,1)}), bf16[32,8,768]{2,1,0:T(8,128)(2,1)S(1)}, u32[]{:S(2)}, u32[]{:S(2)}) %all-to-all-start) | async-done | bytes 393248 | tf_op jit(solution)/shard_map/all_to_all | solution.py:564
  27.2 5.3 %experts.1._ = bf16[256,512]{1,0:T(8,128)(2,1)} custom-call(bf16[8,32,768]{2,1,0:T(8,128)(2,1)S(1)} %bitcast.15, f32[1,2048]{1,0:T(1,128)S(1)} %get-tuple-element.20.gain_ref, bf16[1024,512]{1,0:T(8,128)(2,1)S(1)} %get-tuple-element.21.refs_0_, bf16[1024,2048]{1,0:T(8,128)(2,1)} %refs_1_.1, bf16[2048,512]{1,0:T(8,128)(2,1)} %bitcast.18, ...), custom_call_target="tpu_custom_call" | custom-call | flops 671088640 | bytes 1048576 | tf_op jit(solution)/shard_map/experts/pallas_call | solution.py:601
  32.5 0.0 copy-done
  32.5 0.0 copy-done.1
  32.5 2.6 %all-to-all-start.1 = ((bf16[32,8,512]{2,1,0:T(8,128)(2,1)}), bf16[32,8,512]{2,1,0:T(8,128)(2,1)S(1)}, u32[]{:S(2)}, u32[]{:S(2)}) async-start(bf16[32,8,512]{2,1,0:T(8,128)(2,1)} %bitcast.17), calls=%async_computation.1 | async-start | bytes 524288 | tf_op jit(solution)/shard_map/all_to_all | solution.py:624
  35.1 2.7 %shared.1 = (bf16[32,512]{1,0:T(8,128)(2,1)S(1)}, bf16[32,512]{1,0:T(8,128)(2,1)S(1)}, bf16[32,512]{1,0:T(8,128)(2,1)S(1)}, f32[32,512]{1,0:T(8,128)S(1)}, bf16[64,256]{1,0:T(8,128)(2,1)S(1)}) custom-call(bf16[32,2048]{1,0:T(8,128)(2,1)} %copy-done, f32[32,512]{1,0:T(8,128)} %copy-done.1, bf16[256,512]{1,0:T(8,128)(2,1)} %experts.1._, ...), custom_call_target="tpu_custom_call" | custom-call | flops 50331648 | bytes 1572864 | tf_op jit(solution)/shard_map/shared/pallas_call | solution.py:625
  37.9 0.3 collective-permute-start
  38.2 1.6 %collective-permute-start.1 = (bf16[32,512]{1,0:T(8,128)(2,1)S(1)}, bf16[32,512]{1,0:T(8,128)(2,1)S(1)}, u32[]{:S(2)}, u32[]{:S(2)}) collective-permute-start(bf16[32,512]{1,0:T(8,128)(2,1)S(1)} %get-tuple-element.25), channel_id=1, source_target_pairs={{0,2},{1,3},{2,0},{3,1},{4,6},{5,7},{6,4},{7,5},{8,10},{9,11},{10,... | collective-permute-start | bytes 98312 | tf_op jit(solution)/shard_map/ppermute | solution.py:659
  39.8 0.0 collective-permute-start.2
  39.8 0.0 collective-permute-done.refs_0_
  39.8 2.4 %collective-permute-done.1.refs_1_ = bf16[32,512]{1,0:T(8,128)(2,1)S(1)} collective-permute-done((bf16[32,512]{1,0:T(8,128)(2,1)S(1)}, bf16[32,512]{1,0:T(8,128)(2,1)S(1)}, u32[]{:S(2)}, u32[]{:S(2)}) %collective-permute-start.1) | collective-permute-done | bytes 32800 | tf_op jit(solution)/shard_map/ppermute | solution.py:659
  42.2 1.3 %collective-permute-done.2.refs_2_ = bf16[32,512]{1,0:T(8,128)(2,1)S(1)} collective-permute-done((bf16[32,512]{1,0:T(8,128)(2,1)S(1)}, bf16[32,512]{1,0:T(8,128)(2,1)S(1)}, u32[]{:S(2)}, u32[]{:S(2)}) %collective-permute-start.2) | collective-permute-done | bytes 32800 | tf_op jit(solution)/shard_map/ppermute | solution.py:659
  43.5 2.2 %all-to-all-done.1 = bf16[32,8,512]{2,1,0:T(8,128)(2,1)S(1)} async-done(((bf16[32,8,512]{2,1,0:T(8,128)(2,1)}), bf16[32,8,512]{2,1,0:T(8,128)(2,1)S(1)}, u32[]{:S(2)}, u32[]{:S(2)}) %all-to-all-start.1) | async-done | bytes 262176 | tf_op jit(solution)/shard_map/all_to_all | solution.py:624
  45.7 0.8 %combine.1 = bf16[32,512]{1,0:T(8,128)(2,1)} custom-call(f32[32,512]{1,0:T(8,128)S(1)} %get-tuple-element.22.base_ref, bf16[64,256]{1,0:T(8,128)(2,1)S(1)} %get-tuple-element.23.mix_ref, bf16[256,512]{1,0:T(8,128)(2,1)S(1)} %bitcast.16, bf16[32,512]{1,0:T(8,128)(2,1)S(1)} %collective-permute-done.refs_0_, ...), custom_call_target="tpu_custom_call" | custom-call | tf_op jit(solution)/shard_map/combine/pallas_call | solution.py:663
Async XLA Ops:
  6.6 20.6 %all-to-all-start = ((bf16[32,8,768]{2,1,0:T(8,128)(2,1)}), bf16[32,8,768]{2,1,0:T(8,128)(2,1)S(1)}, u32[]{:S(2)}, u32[]{:S(2)}) async-start(bf16[32,8,768]{2,1,0:T(8,128)(2,1)} %bitcast.21), calls=%async_computation | async-start | bytes 786432 | tf_op jit(solution)/shard_map/all_to_all | solution.py:564
  23.5 9.0 %copy-start = (bf16[32,2048]{1,0:T(8,128)(2,1)}, bf16[32,2048]{1,0:T(8,128)(2,1)S(1)}, u32[]{:S(2)}) copy-start(bf16[32,2048]{1,0:T(8,128)(2,1)S(1)} %get-tuple-element.17.ffn_ref) | copy-start | bytes 393220
  23.5 9.0 %copy-start.1 = (f32[32,512]{1,0:T(8,128)}, f32[32,512]{1,0:T(8,128)S(1)}, u32[]{:S(2)}) copy-start(f32[32,512]{1,0:T(8,128)S(1)} %get-tuple-element.18.residual_ref) | copy-start | bytes 196612
  32.5 13.2 %all-to-all-start.1 = ((bf16[32,8,512]{2,1,0:T(8,128)(2,1)}), bf16[32,8,512]{2,1,0:T(8,128)(2,1)S(1)}, u32[]{:S(2)}, u32[]{:S(2)}) async-start(bf16[32,8,512]{2,1,0:T(8,128)(2,1)} %bitcast.17), calls=%async_computation.1 | async-start | bytes 524288 | tf_op jit(solution)/shard_map/all_to_all | solution.py:624
  37.9 1.9 %collective-permute-start = (bf16[32,512]{1,0:T(8,128)(2,1)S(1)}, bf16[32,512]{1,0:T(8,128)(2,1)S(1)}, u32[]{:S(2)}, u32[]{:S(2)}) collective-permute-start(bf16[32,512]{1,0:T(8,128)(2,1)S(1)} %get-tuple-element.24), channel_id=1, source_target_pairs={{0,1},{1,0},{2,3},{3,2},{4,5},{5,4},{6,7},{7,6},{8,9},{9,8},{10,11... | collective-permute-start | bytes 98312 | tf_op jit(solution)/shard_map/ppermute | solution.py:659
  38.2 4.1 %collective-permute-start.1 = (bf16[32,512]{1,0:T(8,128)(2,1)S(1)}, bf16[32,512]{1,0:T(8,128)(2,1)S(1)}, u32[]{:S(2)}, u32[]{:S(2)}) collective-permute-start(bf16[32,512]{1,0:T(8,128)(2,1)S(1)} %get-tuple-element.25), channel_id=1, source_target_pairs={{0,2},{1,3},{2,0},{3,1},{4,6},{5,7},{6,4},{7,5},{8,10},{9,11},{10,... | collective-permute-start | bytes 98312 | tf_op jit(solution)/shard_map/ppermute | solution.py:659
  39.8 3.7 %collective-permute-start.2 = (bf16[32,512]{1,0:T(8,128)(2,1)S(1)}, bf16[32,512]{1,0:T(8,128)(2,1)S(1)}, u32[]{:S(2)}, u32[]{:S(2)}) collective-permute-start(bf16[32,512]{1,0:T(8,128)(2,1)S(1)} %get-tuple-element.26), channel_id=1, source_target_pairs={{0,3},{1,2},{2,1},{3,0},{4,7},{5,6},{6,5},{7,4},{8,11},{9,10},{10,... | collective-permute-start | bytes 98312 | tf_op jit(solution)/shard_map/ppermute | solution.py:659

commit v6 on v5

--- a/solution.py
+++ b/solution.py
@@ -33,33 +33,37 @@
     return lax.rsqrt(jnp.mean(values * values, axis=-1, keepdims=True) + epsilon)
 
 
-def slots_of(routing, experts, capacity):
+def slots_of(routing, experts, capacity, tp_count):
     rows, top_count = routing.shape
-    ids = iota((rows, experts), 1)
-    hits = [routing[:, k : k + 1] == ids for k in range(top_count)]
+    ids = iota((rows, experts), 1).astype(f32)
+    columns = [routing[:, k : k + 1] for k in range(top_count)]
+    hits = [column == ids for column in columns]
     present = jnp.zeros((rows, experts), f32)
     for hit in hits:
         present = jnp.where(hit, 1.0, present)
     earlier = (iota((rows, rows), 1) < iota((rows, rows), 0)).astype(bf16)
     before = dot(earlier, present.astype(bf16))
-    ranks = [jnp.sum(jnp.where(hit, before, 0.0), axis=1, keepdims=True) for hit in hits]
-    return [
-        routing[:, k : k + 1] * capacity + ranks[k].astype(jnp.int32) for k in range(top_count)
-    ]
-
-
-def own_slots(routing_ref, slot_scr, seqs, experts, capacity):
+    slots = []
+    for column, hit in zip(columns, hits):
+        rank = jnp.sum(jnp.where(hit, before, 0.0), axis=1, keepdims=True)
+        across = jnp.floor((column + 0.5) * (1.0 / tp_count))
+        device = (column - across * tp_count) * (experts // tp_count) + across
+        slots.append((device * capacity + rank).astype(jnp.int32))
+    return slots
+
+
+def own_slots(routing_ref, slot_scr, seqs, experts, capacity, tp_count):
     top_count, batch = routing_ref.shape
     pad = jnp.zeros((8 - top_count, batch), f32)
     slot_scr[...] = jnp.concatenate([routing_ref[...].astype(f32), pad], axis=0).T
     start = pl.multiple_of(lax.axis_index("ep") * seqs, seqs)
-    own = slot_scr[pl.ds(start, seqs), :top_count].astype(jnp.int32)
-    return slots_of(own, experts, capacity)
+    return slots_of(slot_scr[pl.ds(start, seqs), :top_count], experts, capacity, tp_count)
 
 
 def attention_kernel(
     capacity,
     experts,
+    tp_count,
     block,
     tokens_hbm,
     attn_gain_hbm,
@@ -133,7 +137,7 @@
     for stream in streams[1:]:
         stream.start()
 
-    slots = own_slots(routing_ref, slot_scr, seqs, experts, capacity)
+    slots = own_slots(routing_ref, slot_scr, seqs, experts, capacity, tp_count)
     ids = iota((seqs, experts * capacity), 1)
     picks = jnp.zeros((seqs, experts * capacity), f32)
     for slot in slots:
@@ -344,7 +348,7 @@
         copy.start()
     for copy in copies[:2]:
         copy.wait()
-    slots = own_slots(routing_ref, slot_scr, seqs, experts, capacity)
+    slots = own_slots(routing_ref, slot_scr, seqs, experts, capacity, tp_count)
     top_count = rates_ref.shape[0]
     rates = jnp.concatenate([rates_ref[...], jnp.zeros((8 - top_count, seqs), f32)], axis=0)
     rates = jnp.concatenate([rates, jnp.zeros((8, 128 - seqs), f32)], axis=1).T[:seqs]
@@ -379,7 +383,6 @@
 
 
 def expert_kernel(
-    direct,
     kept,
     arrived_ref,
     gain_ref,
@@ -399,6 +402,7 @@
         down_ref,
         res_scr,
         sems,
+        back_sems,
     ) = refs[kept:]
     blocks = column_blocks(w_out_hbm, rest_ref, kept_refs)
     copies = [
@@ -414,19 +418,15 @@
     ]
     for copy in copies:
         copy.start()
-    groups, chunk, packed = arrived_ref.shape
-    rows, model = res_scr.shape
-    capacity = rows // groups
-    tp_count = chunk // capacity
+    tp_count, rows, packed = arrived_ref.shape
+    model = res_scr.shape[1]
     share = model // tp_count
     width = packed - share
     lefts = []
     tokens = []
     for j in range(tp_count):
-        piece = arrived_ref[:, j * capacity : (j + 1) * capacity, :].astype(f32)
-        piece = piece.reshape(rows, packed)
-        lefts.append(piece[:, :width].astype(bf16))
-        tokens.append(piece[:, width:])
+        lefts.append(arrived_ref[j, :, :width])
+        tokens.append(arrived_ref[j, :, width:].astype(f32))
     square = jnp.zeros((rows, 1), f32)
     for n in range(tp_count):
         if n >= kept:
@@ -446,20 +446,15 @@
     gate = dot(ffn_in, gate_ref[...])
     copies[tp_count - kept + 1].wait()
     act = (silu(gate) * dot(ffn_in, up_ref[...])).astype(bf16)
+    backs = []
     for n in range(tp_count):
         copies[n - tp_count].wait()
-        result = dot(act, down_ref[n])
-        if direct:
-            for i in range(groups):
-                first = (i * tp_count + n) * capacity
-                send_ref[first : first + capacity, :] = result[
-                    i * capacity : (i + 1) * capacity
-                ].astype(bf16)
-        else:
-            send_ref[:, n * share : (n + 1) * share] = result.astype(bf16)
-    back = pltpu.make_async_copy(send_ref, send_hbm, sems.at[0])
-    back.start()
-    back.wait()
+        cut = pl.ds(n * rows, rows)
+        send_ref[cut] = dot(act, down_ref[n]).astype(bf16)
+        backs.append(pltpu.make_async_copy(send_ref.at[cut], send_hbm.at[cut], back_sems.at[n]))
+        backs[n].start()
+    for back in backs:
+        back.wait()
 
 
 def combine_kernel(base_ref, mix_ref, returned_ref, *refs):
@@ -511,10 +506,9 @@
     share = width // tp_count
     local = heads * v_width
     packed = local + share
-    direct = capacity % 8 == 0
-    block = 4
+    block = 8
     head_out, send = pl.pallas_call(
-        functools.partial(attention_kernel, capacity, experts, block),
+        functools.partial(attention_kernel, capacity, experts, tp_count, block),
         in_specs=[HBM] * 10,
         out_specs=[VMEM, HBM],
         out_shape=[
@@ -561,8 +555,8 @@
         kv_cache,
     )
 
-    arrived = lax.all_to_all(send, ("ep", "tp"), split_axis=0, concat_axis=0, tiled=True)
-    arrived = arrived.reshape(ep_count, tp_count * capacity, packed)
+    arrived = lax.all_to_all(send, ("tp", "ep"), split_axis=0, concat_axis=0, tiled=True)
+    arrived = arrived.reshape(tp_count, ep_count * capacity, packed)
     all_heads = lax.all_gather(head_out, "tp", axis=0, tiled=False)
 
     exp_gate = w_exp_gate.reshape(w_exp_gate.shape[1:])
@@ -597,9 +591,9 @@
         pltpu.with_memory_space_constraint(value, pltpu.VMEM) for value in (arrived, gain, kept)
     ]
 
-    sent_shape = (devices * capacity, share) if direct else (rows, width)
+    sent_shape = (devices * capacity, share)
     sent = pl.pallas_call(
-        functools.partial(expert_kernel, direct, 1),
+        functools.partial(expert_kernel, 1),
         in_specs=[VMEM] * 3 + [HBM] * 4,
         out_specs=HBM,
         out_shape=jax.ShapeDtypeStruct(sent_shape, bf16),
@@ -611,6 +605,7 @@
             pltpu.VMEM((tp_count, exp_down.shape[0], share), bf16),
             pltpu.VMEM((rows, width), f32),
             pltpu.SemaphoreType.DMA((1 + 2 * tp_count,)),
+            pltpu.SemaphoreType.DMA((tp_count,)),
         ],
         compiler_params=pltpu.CompilerParams(vmem_limit_bytes=60 * 1024 * 1024),
         cost_estimate=pl.CostEstimate(
@@ -618,10 +613,7 @@
         ),
         name="experts",
     )(arrived, gain, kept, w_out, exp_gate, exp_up, exp_down)
-    if not direct:
-        sent = sent.reshape(ep_count, capacity, tp_count, share)
-        sent = sent.transpose(0, 2, 1, 3).reshape(devices * capacity, share)
-    returned = lax.all_to_all(sent, ("ep", "tp"), split_axis=0, concat_axis=0, tiled=True)
+    returned = lax.all_to_all(sent, ("tp", "ep"), split_axis=0, concat_axis=0, tiled=True)
     *part, base, mix = pl.pallas_call(
         functools.partial(shared_kernel, capacity, experts),
         in_specs=[VMEM] * 2 + [HBM] * 6,

time: 46.8 us -> 46.8 us (level)
  no operation moved by 1% of the time
where the time goes in v6:
time: 46.8 us; the launch traced here: 46.4 us
  Pallas kernels  19 us (41%)
  starting transfers between devices  11.9 us (25%)
  waiting for transfers between devices  9.27 us (20%)
  blocking collectives  6.18 us (13%)
    all_to_all x1, starting transfers between devices, shards(): lax.all_to_all(send, ('tp', 'ep'), split_axis=0, concat_axis=0, tiled=True)  7.33 us
    pallas_call x1, Pallas kernels, shards(): pl.pallas_call(functools.partial(attention_kernel, capacity, experts, tp_...  6.39 us
    all_gather x1, blocking collectives, shards(): all_heads = lax.all_gather(head_out, 'tp', axis=0, tiled=False)  6.18 us
    pallas_call x1, Pallas kernels, shards(): pl.pallas_call(functools.partial(expert_kernel, 1), in_specs=[VMEM] * 3 +...  5.41 us
    pallas_call x1, Pallas kernels, shards(): pl.pallas_call(own_kernel, in_specs=[VMEM] + [HBM] * 3, out_specs=[VMEM]...  3.75 us
    ppermute x3, waiting for transfers between devices, shards(): lax.ppermute(piece, 'tp', [(i, partner(i, d, tp_count)) for i in range(tp...  3.58 us
    all_to_all x1, waiting for transfers between devices, shards(): lax.all_to_all(send, ('tp', 'ep'), split_axis=0, concat_axis=0, tiled=True)  3.47 us
    pallas_call x1, Pallas kernels, shards(): pl.pallas_call(functools.partial(shared_kernel, capacity, experts), in_sp...  2.7 us
  transfers between devices with their start and end apart: 5, of which 4 were waited for; matrix products, arithmetic and copies ran while one was open for 0% of the time, Pallas kernels for 14%

profile of v6, /device:TPU:0, one launch (start us, length us, event | category | flops | bytes accessed | tf_op | source)
XLA Modules:
  0.0 46.4 jit_solution(441916764105451249)
XLA Ops:
  0.0 6.4 %attention.1 = (bf16[32,256]{1,0:T(8,128)(2,1)S(1)}, bf16[256,768]{1,0:T(8,128)(2,1)}) custom-call(bf16[32,2048]{1,0:T(8,128)(2,1)} %tokens_hbm.3, f32[1,2048]{1,0:T(1,128)} %bitcast.28, bf16[2048,256]{1,0:T(8,128)(2,1)} %w_query_hbm.1, bf16[64,2048]{1,0:T(8,128)(2,1)} %bitcast.23, bf16[64,2048]{1,0:T(8,128)(2,1)} %bitcast.24, f32[1,64]{1,0:T(1,128)} %bitcast.30, ...), custom_call_target="tpu_custom_call" | custom-call | flops 134217728 | bytes 8388608 | tf_op jit(solution)/shard_map/attention/pallas_call | solution.py:510
  6.4 7.3 %all-to-all-start = ((bf16[32,8,768]{2,1,0:T(8,128)(2,1)}), bf16[32,8,768]{2,1,0:T(8,128)(2,1)S(1)}, u32[]{:S(2)}, u32[]{:S(2)}) async-start(bf16[32,8,768]{2,1,0:T(8,128)(2,1)} %bitcast.21), calls=%async_computation | async-start | bytes 786432 | tf_op jit(solution)/shard_map/all_to_all | solution.py:558
  13.7 6.2 %all-gather = bf16[128,256]{1,0:T(8,128)(2,1)} all-gather(bf16[32,256]{1,0:T(8,128)(2,1)S(1)} %get-tuple-element.16), channel_id=2, replica_groups=mesh['ep'=8,'tp'=4] {'tp'}, dimensions={0}, use_global_device_ids=true | all-gather | bytes 81920 | tf_op jit(solution)/shard_map/all_gather | solution.py:560
  19.9 3.7 %own.1 = (bf16[32,2048]{1,0:T(8,128)(2,1)S(1)}, f32[32,512]{1,0:T(8,128)S(1)}, f32[1,2048]{1,0:T(1,128)S(1)}, bf16[1024,512]{1,0:T(8,128)(2,1)S(1)}) custom-call(bf16[4,32,256]{2,1,0:T(8,128)(2,1)} %bitcast.22, bf16[1024,2048]{1,0:T(8,128)(2,1)} %refs_1_.1, bf16[32,2048]{1,0:T(8,128)(2,1)} %tokens_hbm.3, f32[1,2048]{1,0:T(1,128)} %bitcast.27), custom_call_target="tpu_custom_call" | custom-call | flops 134217728 | bytes 4194304 | tf_op jit(solution)/shard_map/own/pallas_call | solution.py:568
  23.7 0.0 copy-start
  23.7 0.0 copy-start.1
  23.7 3.5 %all-to-all-done = bf16[32,8,768]{2,1,0:T(8,128)(2,1)S(1)} async-done(((bf16[32,8,768]{2,1,0:T(8,128)(2,1)}), bf16[32,8,768]{2,1,0:T(8,128)(2,1)S(1)}, u32[]{:S(2)}, u32[]{:S(2)}) %all-to-all-start) | async-done | bytes 393248 | tf_op jit(solution)/shard_map/all_to_all | solution.py:558
  27.2 5.4 %experts.1._ = bf16[256,512]{1,0:T(8,128)(2,1)} custom-call(bf16[4,64,768]{2,1,0:T(8,128)(2,1)S(1)} %bitcast.15, f32[1,2048]{1,0:T(1,128)S(1)} %get-tuple-element.20.gain_ref, bf16[1024,512]{1,0:T(8,128)(2,1)S(1)} %get-tuple-element.21.refs_0_, bf16[1024,2048]{1,0:T(8,128)(2,1)} %refs_1_.1, bf16[2048,512]{1,0:T(8,128)(2,1)} %bitcast.18, ...), custom_call_target="tpu_custom_call" | custom-call | flops 671088640 | bytes 1048576 | tf_op jit(solution)/shard_map/experts/pallas_call | solution.py:595
  32.6 0.0 copy-done
  32.6 0.0 copy-done.1
  32.6 2.6 %all-to-all-start.1 = ((bf16[32,8,512]{2,1,0:T(8,128)(2,1)}), bf16[32,8,512]{2,1,0:T(8,128)(2,1)S(1)}, u32[]{:S(2)}, u32[]{:S(2)}) async-start(bf16[32,8,512]{2,1,0:T(8,128)(2,1)} %bitcast.17), calls=%async_computation.1 | async-start | bytes 524288 | tf_op jit(solution)/shard_map/all_to_all | solution.py:616
  35.2 2.7 %shared.1 = (bf16[32,512]{1,0:T(8,128)(2,1)S(1)}, bf16[32,512]{1,0:T(8,128)(2,1)S(1)}, bf16[32,512]{1,0:T(8,128)(2,1)S(1)}, f32[32,512]{1,0:T(8,128)S(1)}, bf16[64,256]{1,0:T(8,128)(2,1)S(1)}) custom-call(bf16[32,2048]{1,0:T(8,128)(2,1)} %copy-done, f32[32,512]{1,0:T(8,128)} %copy-done.1, bf16[256,512]{1,0:T(8,128)(2,1)} %experts.1._, ...), custom_call_target="tpu_custom_call" | custom-call | flops 50331648 | bytes 1572864 | tf_op jit(solution)/shard_map/shared/pallas_call | solution.py:617
  37.9 0.2 collective-permute-start
  38.1 1.6 %collective-permute-start.1 = (bf16[32,512]{1,0:T(8,128)(2,1)S(1)}, bf16[32,512]{1,0:T(8,128)(2,1)S(1)}, u32[]{:S(2)}, u32[]{:S(2)}) collective-permute-start(bf16[32,512]{1,0:T(8,128)(2,1)S(1)} %get-tuple-element.25), channel_id=1, source_target_pairs={{0,2},{1,3},{2,0},{3,1},{4,6},{5,7},{6,4},{7,5},{8,10},{9,11},{10,... | collective-permute-start | bytes 98312 | tf_op jit(solution)/shard_map/ppermute | solution.py:651
  39.8 0.1 collective-permute-start.2
  39.9 0.0 collective-permute-done.refs_0_
  39.9 2.3 %collective-permute-done.1.refs_1_ = bf16[32,512]{1,0:T(8,128)(2,1)S(1)} collective-permute-done((bf16[32,512]{1,0:T(8,128)(2,1)S(1)}, bf16[32,512]{1,0:T(8,128)(2,1)S(1)}, u32[]{:S(2)}, u32[]{:S(2)}) %collective-permute-start.1) | collective-permute-done | bytes 32800 | tf_op jit(solution)/shard_map/ppermute | solution.py:651
  42.1 1.3 %collective-permute-done.2.refs_2_ = bf16[32,512]{1,0:T(8,128)(2,1)S(1)} collective-permute-done((bf16[32,512]{1,0:T(8,128)(2,1)S(1)}, bf16[32,512]{1,0:T(8,128)(2,1)S(1)}, u32[]{:S(2)}, u32[]{:S(2)}) %collective-permute-start.2) | collective-permute-done | bytes 32800 | tf_op jit(solution)/shard_map/ppermute | solution.py:651
  43.4 2.2 %all-to-all-done.1 = bf16[32,8,512]{2,1,0:T(8,128)(2,1)S(1)} async-done(((bf16[32,8,512]{2,1,0:T(8,128)(2,1)}), bf16[32,8,512]{2,1,0:T(8,128)(2,1)S(1)}, u32[]{:S(2)}, u32[]{:S(2)}) %all-to-all-start.1) | async-done | bytes 262176 | tf_op jit(solution)/shard_map/all_to_all | solution.py:616
  45.7 0.8 %combine.1 = bf16[32,512]{1,0:T(8,128)(2,1)} custom-call(f32[32,512]{1,0:T(8,128)S(1)} %get-tuple-element.22.base_ref, bf16[64,256]{1,0:T(8,128)(2,1)S(1)} %get-tuple-element.23.mix_ref, bf16[256,512]{1,0:T(8,128)(2,1)S(1)} %bitcast.16, bf16[32,512]{1,0:T(8,128)(2,1)S(1)} %collective-permute-done.refs_0_, ...), custom_call_target="tpu_custom_call" | custom-call | tf_op jit(solution)/shard_map/combine/pallas_call | solution.py:655
Async XLA Ops:
  6.4 20.8 %all-to-all-start = ((bf16[32,8,768]{2,1,0:T(8,128)(2,1)}), bf16[32,8,768]{2,1,0:T(8,128)(2,1)S(1)}, u32[]{:S(2)}, u32[]{:S(2)}) async-start(bf16[32,8,768]{2,1,0:T(8,128)(2,1)} %bitcast.21), calls=%async_computation | async-start | bytes 786432 | tf_op jit(solution)/shard_map/all_to_all | solution.py:558
  23.7 8.9 %copy-start = (bf16[32,2048]{1,0:T(8,128)(2,1)}, bf16[32,2048]{1,0:T(8,128)(2,1)S(1)}, u32[]{:S(2)}) copy-start(bf16[32,2048]{1,0:T(8,128)(2,1)S(1)} %get-tuple-element.17.ffn_ref) | copy-start | bytes 393220
  23.7 8.9 %copy-start.1 = (f32[32,512]{1,0:T(8,128)}, f32[32,512]{1,0:T(8,128)S(1)}, u32[]{:S(2)}) copy-start(f32[32,512]{1,0:T(8,128)S(1)} %get-tuple-element.18.residual_ref) | copy-start | bytes 196612
  32.6 13.0 %all-to-all-start.1 = ((bf16[32,8,512]{2,1,0:T(8,128)(2,1)}), bf16[32,8,512]{2,1,0:T(8,128)(2,1)S(1)}, u32[]{:S(2)}, u32[]{:S(2)}) async-start(bf16[32,8,512]{2,1,0:T(8,128)(2,1)} %bitcast.17), calls=%async_computation.1 | async-start | bytes 524288 | tf_op jit(solution)/shard_map/all_to_all | solution.py:616
  37.9 1.9 %collective-permute-start = (bf16[32,512]{1,0:T(8,128)(2,1)S(1)}, bf16[32,512]{1,0:T(8,128)(2,1)S(1)}, u32[]{:S(2)}, u32[]{:S(2)}) collective-permute-start(bf16[32,512]{1,0:T(8,128)(2,1)S(1)} %get-tuple-element.24), channel_id=1, source_target_pairs={{0,1},{1,0},{2,3},{3,2},{4,5},{5,4},{6,7},{7,6},{8,9},{9,8},{10,11... | collective-permute-start | bytes 98312 | tf_op jit(solution)/shard_map/ppermute | solution.py:651
  38.1 4.0 %collective-permute-start.1 = (bf16[32,512]{1,0:T(8,128)(2,1)S(1)}, bf16[32,512]{1,0:T(8,128)(2,1)S(1)}, u32[]{:S(2)}, u32[]{:S(2)}) collective-permute-start(bf16[32,512]{1,0:T(8,128)(2,1)S(1)} %get-tuple-element.25), channel_id=1, source_target_pairs={{0,2},{1,3},{2,0},{3,1},{4,6},{5,7},{6,4},{7,5},{8,10},{9,11},{10,... | collective-permute-start | bytes 98312 | tf_op jit(solution)/shard_map/ppermute | solution.py:651
  39.8 3.7 %collective-permute-start.2 = (bf16[32,512]{1,0:T(8,128)(2,1)S(1)}, bf16[32,512]{1,0:T(8,128)(2,1)S(1)}, u32[]{:S(2)}, u32[]{:S(2)}) collective-permute-start(bf16[32,512]{1,0:T(8,128)(2,1)S(1)} %get-tuple-element.26), channel_id=1, source_target_pairs={{0,3},{1,2},{2,1},{3,0},{4,7},{5,6},{6,5},{7,4},{8,11},{9,10},{10,... | collective-permute-start | bytes 98312 | tf_op jit(solution)/shard_map/ppermute | solution.py:651
